TPU v7x, 32 devices: a whole 2x2x4 slice. The times are simulated.
32 devices in a mesh: ep: 8 (over z, x), tp: 4 (over y, core).
Axes of the slice: x: 2, y: 2, z: 4, core: 2. Of those that a mesh axis runs over, the one named last changes fastest.
Arguments:
- tokens: bfloat16 [2048, 2048], P('ep'), may hold values from -6 to 6
- routes: int32 [2048, 2], P('ep'), may hold values from 0 to 7, all different within a row; in each aligned block of 256 rows (0 to 255, 256 to 511, ...) at most 128 rows name the same one
- router_matrix: bfloat16 [2048, 8], replicated, may hold values from -0.125 to 0.125
- cotangent: bfloat16 [2048, 2048], P('ep', 'tp'), may hold values from -3 to 3
- gate_proj: bfloat16 [8, 2048, 3584], P('ep', None, 'tp'), may hold values from -0.125 to 0.125
- up_proj: bfloat16 [8, 2048, 3584], P('ep', None, 'tp'), may hold values from -0.125 to 0.125
- down_proj: bfloat16 [8, 3584, 2048], P('ep', 'tp'), may hold values from -0.09375 to 0.09375
Outputs:
- token_grad: bfloat16 [2048, 2048], P('ep', 'tp')
- mixing_grad: float32 [2048, 2], P('ep')
- router_grad: float32 [2048, 8], P(('ep', 'tp'))
- gate_grad: bfloat16 [8, 2048, 3584], P('ep', None, 'tp')
- up_grad: bfloat16 [8, 2048, 3584], P('ep', None, 'tp')
- down_grad: bfloat16 [8, 3584, 2048], P('ep', 'tp')
Inputs may be any that keep to these rules, and one draw needn't show every extreme that they name: `routes`: the two experts of a row differ. In each aligned block of 256 rows no expert is named by more than 128 rows, a bound that some block reaches; every expert is named somewhere.
All inputs are finite; a program needn't handle non-finite values.
Results may differ from a plain program's by a relative error of at most 0.019.
Values may be sent and summed in bfloat16 or wider, within the bound.
A program may use at most 128 MiB of HBM per device.

v0:
```python
import math

import jax
import jax.numpy as jnp
from jax import lax
from jax.sharding import PartitionSpec as P


def slot_places(flat_routes, experts, capacity):
    onehot = (flat_routes[:, None] == jnp.arange(experts, dtype=jnp.int32)[None, :]).astype(
        jnp.int32
    )
    earlier = jnp.cumsum(onehot, axis=0) - onehot
    places = flat_routes * capacity + jnp.sum(earlier * onehot, axis=1)
    entries = flat_routes.shape[0]
    filler = (
        jnp.full((experts * capacity,), entries, jnp.int32)
        .at[places]
        .set(jnp.arange(entries, dtype=jnp.int32))
    )
    return (places, filler)


def local(tokens, routes, router_matrix, cotangent, gate_proj, up_proj, down_proj):
    ep_size = lax.axis_size("ep")
    tp_size = lax.axis_size("tp")
    tp_index = lax.axis_index("tp")
    home_rows, model_width = tokens.shape
    top_count = routes.shape[1]
    experts = router_matrix.shape[1]
    capacity = home_rows * top_count * 2 // experts
    entries = home_rows * top_count
    col_width = model_width // tp_size
    places, filler = slot_places(routes.reshape(-1), experts, capacity)
    occupied = filler < entries
    source = jnp.where(occupied, filler // top_count, 0)
    entry_src = jnp.where(occupied, filler, 0)
    logits = jnp.dot(tokens, router_matrix, preferred_element_type=jnp.float32)
    picked = routes[:, :, None] == jnp.arange(experts, dtype=jnp.int32)[None, None, :]
    chosen = jnp.sum(jnp.where(picked, logits[:, None, :], 0.0), axis=2)
    mixing = jax.nn.sigmoid(chosen - chosen[:, ::-1])
    mix_send = (
        jnp.where(occupied, mixing.reshape(-1)[entry_src], 0.0)
        .astype(jnp.bfloat16)
        .reshape(experts, capacity)
    )
    zero_value = jnp.zeros((), jnp.bfloat16)
    token_cols = lax.dynamic_slice_in_dim(tokens, tp_index * col_width, col_width, 1)
    token_send = jnp.where(occupied[:, None], token_cols[source], zero_value).reshape(
        experts, capacity, col_width
    )
    output_send = jnp.where(occupied[:, None], cotangent[source], zero_value).reshape(
        experts, capacity, col_width
    )
    token_part_in, output_part_in, mix_in = (
        lax.all_to_all(token_send, "ep", split_axis=0, concat_axis=0, tiled=True),
        lax.all_to_all(output_send, "ep", split_axis=0, concat_axis=0, tiled=True),
        lax.all_to_all(mix_send, "ep", split_axis=0, concat_axis=0, tiled=True),
    )
    token_in, output_in = (
        lax.all_gather(token_part_in, "tp", axis=2, tiled=True),
        lax.all_gather(output_part_in, "tp", axis=2, tiled=True),
    )
    senders = token_in.shape[0]
    slots = senders * capacity
    token_rows = token_in.reshape(slots, model_width)
    output_rows = output_in.reshape(slots, model_width)
    mix_value = mix_in.reshape(slots).astype(jnp.float32)
    w_gate = gate_proj[0]
    w_up = up_proj[0]
    w_down = down_proj[0]
    over_rows = (((0,), (0,)), ((), ()))
    over_cols = (((1,), (1,)), ((), ()))
    gate_pre = jnp.dot(token_rows, w_gate, preferred_element_type=jnp.float32)
    up_pre = jnp.dot(token_rows, w_up, preferred_element_type=jnp.float32)
    gate_sig = jax.nn.sigmoid(gate_pre)
    active = gate_pre * gate_sig
    hidden = (active * up_pre).astype(jnp.bfloat16)
    back_hidden = lax.dot_general(
        output_rows, w_down, over_cols, preferred_element_type=jnp.float32
    )
    mix_part = jnp.sum(hidden.astype(jnp.float32) * back_hidden, axis=1)
    scaled = mix_value[:, None] * back_hidden
    gate_back = (scaled * up_pre * gate_sig * (1.0 + gate_pre * (1.0 - gate_sig))).astype(
        jnp.bfloat16
    )
    up_back = (scaled * active).astype(jnp.bfloat16)
    out_scaled = (mix_value[:, None] * output_rows).astype(jnp.bfloat16)
    gate_grad = lax.dot_general(
        token_rows, gate_back, over_rows, preferred_element_type=jnp.float32
    ).astype(jnp.bfloat16)[None]
    up_grad = lax.dot_general(
        token_rows, up_back, over_rows, preferred_element_type=jnp.float32
    ).astype(jnp.bfloat16)[None]
    down_grad = lax.dot_general(
        hidden, out_scaled, over_rows, preferred_element_type=jnp.float32
    ).astype(jnp.bfloat16)[None]
    slot_terms = lax.dot_general(gate_back, w_gate, over_cols, preferred_element_type=jnp.float32)
    slot_terms = slot_terms + lax.dot_general(
        up_back, w_up, over_cols, preferred_element_type=jnp.float32
    )
    summed = lax.psum_scatter(
        slot_terms.reshape(senders, capacity, model_width).astype(jnp.bfloat16),
        "tp",
        scatter_dimension=2,
        tiled=True,
    )
    mix_total = lax.psum(mix_part.reshape(senders, capacity), "tp")
    back_rows = lax.all_to_all(summed, "ep", split_axis=0, concat_axis=0, tiled=True)
    back_mix = lax.all_to_all(mix_total, "ep", split_axis=0, concat_axis=0, tiled=True)
    back_flat = back_rows.reshape(experts * capacity, col_width)
    token_part = jnp.sum(
        back_flat[places].reshape(home_rows, top_count, col_width).astype(jnp.float32), axis=1
    )
    mixing_grad = back_mix.reshape(-1)[places].reshape(home_rows, top_count)
    pairwise = mixing[:, 0] * mixing[:, 1]
    logit_grad = pairwise[:, None] * (mixing_grad - mixing_grad[:, ::-1])
    route_grad = jnp.sum(jnp.where(picked, logit_grad[:, :, None], 0.0), axis=1)
    router_cols = lax.dynamic_slice_in_dim(
        router_matrix, tp_index * col_width, col_width, 0
    ).astype(jnp.float32)
    router_path = jnp.dot(route_grad, router_cols.T, precision=lax.Precision.HIGHEST)
    token_grad = (token_part + router_path).astype(jnp.bfloat16)
    row_share = model_width // (ep_size * tp_size)
    feature_share = lax.dynamic_slice_in_dim(
        tokens.reshape(home_rows, ep_size, tp_size, row_share), tp_index, 1, 2
    )
    feature_share = feature_share.reshape(home_rows, ep_size * row_share).astype(jnp.float32)
    norm_scale = 1.0 / math.sqrt(home_rows * ep_size)
    router_grad = lax.psum_scatter(
        (jnp.dot(feature_share.T, route_grad, precision=lax.Precision.HIGHEST) * norm_scale).astype(
            jnp.bfloat16
        ),
        "ep",
        scatter_dimension=0,
        tiled=True,
    ).astype(jnp.float32)
    return (token_grad, mixing_grad, router_grad, gate_grad, up_grad, down_grad)


def solution(mesh):
    return jax.shard_map(
        local,
        mesh=mesh,
        in_specs=(
            P("ep", None),
            P("ep", None),
            P(),
            P("ep", "tp"),
            P("ep", None, "tp"),
            P("ep", None, "tp"),
            P("ep", "tp", None),
        ),
        out_specs=(
            P("ep", "tp"),
            P("ep", None),
            P(("ep", "tp"), None),
            P("ep", None, "tp"),
            P("ep", None, "tp"),
            P("ep", "tp", None),
        ),
        check_vma=False,
    )
```

profile of v0, /device:TPU:0, one launch (start us, length us, event | category | flops | bytes accessed | tf_op | source)
XLA Modules:
  0.0 288.1 jit_solution(13943546286839180558)
XLA Ops:
  7.2 0.0 copy-start
  7.2 0.0 all-gather.5.cloned.1.call-start
  7.2 0.7 broadcast_multiply_fusion
  8.0 0.8 copy.34
  8.8 0.1 eq.42
  8.9 0.1 eq.38
  9.1 0.1 copy.33
  9.2 0.1 mul.85
  9.4 1.1 reduce-window.6
  10.5 0.2 slice_reduce_fusion
  10.8 0.1 fusion.15
  10.9 2.4 scatter_custom_fusion
  13.4 1.0 constant_dynamic-slice_fusion.1
  14.3 4.0 %gather_fusion.2 = bf16[1024,512]{1,0:T(8,128)(2,1)S(1)} fusion(bf16[256,512]{1,0:T(8,128)(2,1)S(1)} %constant_dynamic-slice_fusion.1, s32[1024]{0:T(1024)S(1)} %get-tuple-element.29), kind=kCustom, calls=%fused_computation.2 | custom fusion | bytes 2101248 | tf_op jit(solution)/shard_map/gather | solution.py:49
  18.3 4.0 %gather_fusion.1 = bf16[1024,512]{1,0:T(8,128)(2,1)S(1)} fusion(bf16[256,512]{1,0:T(8,128)(2,1)S(1)} %copy-done, s32[1024]{0:T(1024)S(1)} %get-tuple-element.29), kind=kCustom, calls=%fused_computation.1 | custom fusion | bytes 2101248 | tf_op jit(solution)/shard_map/gather | solution.py:52
  22.3 1.2 broadcast_select_fusion.1
  23.5 33.1 %all_to_all.33 = bf16[8,128,512]{2,1,0:T(8,128)(2,1)} all-to-all(bf16[8,128,512]{2,1,0:T(8,128)(2,1)S(1)} %get-tuple-element.31), channel_id=1, replica_groups=mesh['ep'=8,'tp'=4] {'ep'}, dimensions={0} | all-to-all | bytes 2097152 | tf_op jit(solution)/shard_map/all_to_all | solution.py:56
  56.6 0.0 all-gather.5.cloned.1.call-update
  56.6 0.0 all-gather.3.cloned.1.call-start
  56.7 29.0 %all_to_all.34 = bf16[8,128,512]{2,1,0:T(8,128)(2,1)} all-to-all(bf16[8,128,512]{2,1,0:T(8,128)(2,1)S(1)} %copy-done.3), channel_id=1, replica_groups=mesh['ep'=8,'tp'=4] {'ep'}, dimensions={0} | all-to-all | bytes 2097152 | tf_op jit(solution)/shard_map/all_to_all | solution.py:57
  85.6 0.0 all-gather.3.cloned.1.call-update
  85.7 0.0 reduce-scatter.5.cloned.1.call-start
  85.7 0.4 fusion.28
  86.1 0.1 rev.6
  86.3 0.1 copy.36
  86.4 0.2 reshape.124
  86.6 6.8 %gather_fusion = bf16[1024]{0:T(1024)(128)(2,1)S(1)} fusion(bf16[512]{0:T(512)(128)(2,1)S(1)} %reshape.124, s32[1024]{0:T(1024)S(1)} %get-tuple-element.28), kind=kCustom, calls=%fused_computation | custom fusion | bytes 8192 | tf_op jit(solution)/shard_map/gather | solution.py:43
  93.4 9.8 %all_to_all.35 = bf16[8,1,128]{2,1,0:T(2,128)(2,1)S(1)} all-to-all(bf16[8,1,128]{2,1,0:T(2,128)(2,1)S(1)} %copy.37), channel_id=1, replica_groups=mesh['ep'=8,'tp'=4] {'ep'}, dimensions={0} | all-to-all | bytes 4096 | tf_op jit(solution)/shard_map/all_to_all | solution.py:58
  103.2 0.0 copy-start.8
  103.3 9.3 %fusion.4 = f32[1024,896]{0,1:T(8,128)} fusion(bf16[1024,2048]{1,0:T(8,128)(2,1)} %bitcast.78, bf16[1,2048,896]{2,1,0:T(8,128)(2,1)} %param.11), kind=kOutput, calls=%fused_computation.12 | convolution fusion | flops 3758096384 | bytes 11534336 | tf_op jit(solution)/shard_map/dot_general | solution.py:74
  112.6 6.0 %fusion.7 = f32[1024,896]{0,1:T(8,128)} fusion(bf16[1024,2048]{1,0:T(8,128)(2,1)S(1)} %bitcast.81, bf16[1,2048,896]{2,1,0:T(8,128)(2,1)S(1)} %copy-done.8), kind=kOutput, calls=%fused_computation.15 | convolution fusion | flops 3758096384 | bytes 11534336 | tf_op jit(solution)/shard_map/dot_general | solution.py:75
  118.6 7.8 %all-gather.3.cloned.1.call-done = bf16[8,128,2048]{2,1,0:T(8,128)(2,1)} async-done(((bf16[8,128,512]{2,1,0:T(8,128)(2,1)}), bf16[8,128,2048]{2,1,0:T(8,128)(2,1)}) %all-gather.3.cloned.1.call-update) | async-done | bytes 4194320 | tf_op jit(solution)/shard_map/all_gather | solution.py:62
  126.3 12.6 %multiply_reduce_fusion = (f32[1024]{0:T(1024)S(1)}, bf16[1024,896]{0,1:T(8,128)(2,1)}, bf16[1024,896]{0,1:T(8,128)(2,1)S(1)}, bf16[1024,896]{0,1:T(8,128)(2,1)S(1)}) fusion(f32[1024,896]{0,1:T(8,128)} %fusion.7, f32[1024,896]{0,1:T(8,128)} %fusion.4, f32[1024]{0:T(1024)S(1)} %bitcast.75, bf16[1024,2048]{1,0:T(8,128)(2,1)} %bitcast.82, ...), kind=kOutput, calls=%fused_computation.22 | convolution fusion | flops 3775527936 | bytes 20717568 | tf_op jit(solution)/shard_map/dot_general | solution.py:79
  139.0 0.0 copy-start.9
  139.0 4.6 %fusion.2 = f32[1024,2048]{1,0:T(8,128)S(1)} fusion(bf16[1024,896]{0,1:T(8,128)(2,1)S(1)} %get-tuple-element.26, bf16[1,2048,896]{2,1,0:T(8,128)(2,1)S(1)} %copy-done.7), kind=kOutput, calls=%fused_computation.10 | convolution fusion | flops 3758096384 | bytes 13893632 | tf_op jit(solution)/shard_map/dot_general | solution.py:98
  143.6 6.1 %add_convert_fusion = bf16[1024,2048]{1,0:T(8,128)(2,1)} fusion(f32[1024,2048]{1,0:T(8,128)S(1)} %fusion.2, bf16[1024,896]{0,1:T(8,128)(2,1)S(1)} %get-tuple-element.27, bf16[1,2048,896]{2,1,0:T(8,128)(2,1)S(1)} %copy-done.9), kind=kOutput, calls=%fused_computation.7 | convolution fusion | flops 3762290688 | bytes 18087936 | tf_op jit(solution)/shard_map/dot_general | solution.py:99
  149.7 0.0 reduce-scatter.5.cloned.1.call-update
  149.7 0.5 copy.39
  150.3 6.5 %psum.7 = f32[8,1,128]{2,1,0:T(1,128)} all-reduce(f32[8,1,128]{2,1,0:T(1,128)S(1)} %bitcast.77), channel_id=1, replica_groups=mesh['ep'=8,'tp'=4] {'tp'}, use_global_device_ids=true, to_apply=%region_8.9 | all-reduce | flops 1024 | bytes 8192 | tf_op jit(solution)/shard_map/psum | solution.py:108
  156.8 5.7 %all-to-all-start.4 = ((f32[8,1,128]{2,1,0:T(1,128)}), f32[8,1,128]{2,1,0:T(1,128)S(1)}, u32[]{:S(2)}, u32[]{:S(2)}) async-start(f32[8,1,128]{2,1,0:T(1,128)} %psum.7), calls=%async_computation.5 | async-start | bytes 8192 | tf_op jit(solution)/shard_map/all_to_all | solution.py:110
  162.5 8.8 %convert_bitcast_fusion = bf16[1,896,2048]{2,1,0:T(8,128)(2,1)} fusion(bf16[1024,896]{0,1:T(8,128)(2,1)} %get-tuple-element.25, bf16[1024,2048]{1,0:T(8,128)(2,1)} %bitcast.83, f32[1024]{0:T(1024)S(1)} %bitcast.76), kind=kOutput, calls=%fused_computation.19 | convolution fusion | flops 3766222848 | bytes 9703424 | tf_op jit(solution)/shard_map/dot_general | solution.py:95
  171.3 0.0 all-to-all-done.4
  171.3 23.0 %reduce-scatter.5.cloned.1.call-done = bf16[8,128,512]{2,1,0:T(8,128)(2,1)} async-done(((bf16[8,128,2048]{2,1,0:T(8,128)(2,1)}), bf16[8,128,512]{2,1,0:T(8,128)(2,1)}) %reduce-scatter.5.cloned.1.call-update) | async-done | bytes 1048592 | tf_op jit(solution)/shard_map/reduce_scatter | solution.py:102
  194.3 5.5 %all-to-all-start.3 = ((bf16[8,128,512]{2,1,0:T(8,128)(2,1)}), bf16[8,128,512]{2,1,0:T(8,128)(2,1)S(1)}, u32[]{:S(2)}, u32[]{:S(2)}) async-start(bf16[8,128,512]{2,1,0:T(8,128)(2,1)} %reduce-scatter.5.cloned.1.call-done), calls=%async_computation.4 | async-start | bytes 2097152 | tf_op jit(solution)/shard_map/all_to_all | solution.py:109
  199.8 0.0 reduce-scatter.7.cloned.1.call-start
  199.9 8.4 %convert_bitcast_fusion.2 = bf16[1,2048,896]{2,1,0:T(8,128)(2,1)} fusion(bf16[1024,2048]{1,0:T(8,128)(2,1)} %bitcast.79, bf16[1024,896]{0,1:T(8,128)(2,1)S(1)} %copy-done.11), kind=kOutput, calls=%fused_computation.21 | convolution fusion | flops 3759931392 | bytes 9699328 | tf_op jit(solution)/shard_map/dot_general | solution.py:89
  208.3 2.3 gather_fusion.4
  210.6 0.1 reshape.130
  210.7 0.2 rev.7
  210.9 0.1 subtract_multiply_fusion
  211.1 0.1 copy.38
  211.1 0.3 fusion.13
  211.5 0.8 copy.41
  212.3 0.0 reduce-scatter.7.cloned.1.call-update
  212.3 9.2 %convert_bitcast_fusion.1 = bf16[1,2048,896]{2,1,0:T(8,128)(2,1)} fusion(bf16[1024,2048]{1,0:T(8,128)(2,1)} %bitcast.80, bf16[1024,896]{0,1:T(8,128)(2,1)} %copy-done.12), kind=kOutput, calls=%fused_computation.20 | convolution fusion | flops 3759931392 | bytes 9699328 | tf_op jit(solution)/shard_map/dot_general | solution.py:92
  221.5 0.7 copy.40
  222.2 52.5 %reduce-scatter.7.cloned.1.call-done = bf16[64,8]{1,0:T(8,128)(2,1)} async-done(((bf16[512,8]{1,0:T(8,128)(2,1)}), bf16[64,8]{1,0:T(8,128)(2,1)}) %reduce-scatter.7.cloned.1.call-update) | async-done | bytes 1040
  274.7 0.8 copy.42
  275.5 0.6 convert_element_type.85
  276.1 0.0 all-to-all-done.3
  276.1 2.0 gather_fusion.3
  278.1 0.7 reshape.135
  278.7 1.2 reduce_sum.50
  280.0 1.1 fusion.12
  (40 shorter events, 0.2 us)
Async XLA Ops:
  7.2 11.2 %copy-start = (bf16[256,512]{1,0:T(8,128)(2,1)S(1)}, bf16[256,512]{1,0:T(8,128)(2,1)}, u32[]{:S(2)}) copy-start(bf16[256,512]{1,0:T(8,128)(2,1)} %param.10) | copy-start | bytes 786436
  7.2 96.1 %all-gather.5.cloned.1.call-start = ((), (), s32[]{:S(2)}) async-start(), calls=%async_computation.8 | async-start | bytes 5242880 | tf_op jit(solution)/shard_map/all_gather | solution.py:61
  23.5 33.2 %copy-start.3 = (bf16[8,128,512]{2,1,0:T(8,128)(2,1)S(1)}, bf16[8,128,512]{2,1,0:T(8,128)(2,1)}, u32[]{:S(2)}) copy-start(bf16[8,128,512]{2,1,0:T(8,128)(2,1)} %get-tuple-element.30) | copy-start | bytes 3145732
  23.5 62.2 %copy-start.2 = (bf16[256,2048]{1,0:T(8,128)(2,1)S(1)}, bf16[256,2048]{1,0:T(8,128)(2,1)}, u32[]{:S(2)}) copy-start(bf16[256,2048]{1,0:T(8,128)(2,1)} %param.7) | copy-start | bytes 3145732
  23.5 62.2 %copy-start.4 = (bf16[2048,8]{0,1:T(8,128)(2,1)S(1)}, bf16[2048,8]{0,1:T(8,128)(2,1)}, u32[]{:S(2)}) copy-start(bf16[2048,8]{0,1:T(8,128)(2,1)} %param.9) | copy-start | bytes 98308
  23.5 62.6 %copy-start.5 = (s32[256,2]{0,1:T(2,128)S(1)}, s32[256,2]{0,1:T(2,128)}, u32[]{:S(2)}) copy-start(s32[256,2]{0,1:T(2,128)} %param.8) | copy-start | bytes 6148
  56.6 69.7 %all-gather.3.cloned.1.call-start = ((), (), s32[]{:S(2)}) async-start(), calls=%async_computation.7 | async-start | bytes 5242880 | tf_op jit(solution)/shard_map/all_gather | solution.py:62
  85.7 108.6 %reduce-scatter.5.cloned.1.call-start = ((), (), s32[]{:S(2)}) async-start(), calls=%async_computation.9 | async-start | bytes 5242880 | tf_op jit(solution)/shard_map/reduce_scatter | solution.py:102
  103.2 9.3 %copy-start.6 = (bf16[8,128,2048]{2,1,0:T(8,128)(2,1)S(1)}, bf16[8,128,2048]{2,1,0:T(8,128)(2,1)}, u32[]{:S(2)}) copy-start(bf16[8,128,2048]{2,1,0:T(8,128)(2,1)} %all-gather.5.cloned.1.call-done) | copy-start | bytes 12582916
  103.2 9.3 %copy-start.8 = (bf16[1,2048,896]{2,1,0:T(8,128)(2,1)S(1)}, bf16[1,2048,896]{2,1,0:T(8,128)(2,1)}, u32[]{:S(2)}) copy-start(bf16[1,2048,896]{2,1,0:T(8,128)(2,1)} %param.12) | copy-start | bytes 11010052
  126.3 12.6 %copy-start.7 = (bf16[1,2048,896]{2,1,0:T(8,128)(2,1)S(1)}, bf16[1,2048,896]{2,1,0:T(8,128)(2,1)}, u32[]{:S(2)}) copy-start(bf16[1,2048,896]{2,1,0:T(8,128)(2,1)} %param.11) | copy-start | bytes 11010052
  139.0 4.6 %copy-start.10 = (bf16[1024,896]{0,1:T(8,128)(2,1)}, bf16[1024,896]{0,1:T(8,128)(2,1)S(1)}, u32[]{:S(2)}) copy-start(bf16[1024,896]{0,1:T(8,128)(2,1)S(1)} %get-tuple-element.26) | copy-start | bytes 5505028
  139.0 4.6 %copy-start.12 = (bf16[1024,896]{0,1:T(8,128)(2,1)}, bf16[1024,896]{0,1:T(8,128)(2,1)S(1)}, u32[]{:S(2)}) copy-start(bf16[1024,896]{0,1:T(8,128)(2,1)S(1)} %get-tuple-element.27) | copy-start | bytes 5505028
  139.0 4.6 %copy-start.9 = (bf16[1,2048,896]{2,1,0:T(8,128)(2,1)S(1)}, bf16[1,2048,896]{2,1,0:T(8,128)(2,1)}, u32[]{:S(2)}) copy-start(bf16[1,2048,896]{2,1,0:T(8,128)(2,1)} %param.12) | copy-start | bytes 11010052
  156.8 14.4 %all-to-all-start.4 = ((f32[8,1,128]{2,1,0:T(1,128)}), f32[8,1,128]{2,1,0:T(1,128)S(1)}, u32[]{:S(2)}, u32[]{:S(2)}) async-start(f32[8,1,128]{2,1,0:T(1,128)} %psum.7), calls=%async_computation.5 | async-start | bytes 8192 | tf_op jit(solution)/shard_map/all_to_all | solution.py:110
  162.5 37.4 %copy-start.11 = (bf16[1024,896]{0,1:T(8,128)(2,1)S(1)}, bf16[1024,896]{0,1:T(8,128)(2,1)}, u32[]{:S(2)}) copy-start(bf16[1024,896]{0,1:T(8,128)(2,1)} %copy-done.10) | copy-start | bytes 5505028
  194.3 81.8 %all-to-all-start.3 = ((bf16[8,128,512]{2,1,0:T(8,128)(2,1)}), bf16[8,128,512]{2,1,0:T(8,128)(2,1)S(1)}, u32[]{:S(2)}, u32[]{:S(2)}) async-start(bf16[8,128,512]{2,1,0:T(8,128)(2,1)} %reduce-scatter.5.cloned.1.call-done), calls=%async_computation.4 | async-start | bytes 2097152 | tf_op jit(solution)/shard_map/all_to_all | solution.py:109
  199.8 74.9 %reduce-scatter.7.cloned.1.call-start = ((), (), s32[]{:S(2)}) async-start(), calls=%async_computation.10 | async-start | bytes 147456
  276.1 5.0 %copy-start.1 = (bf16[256,512]{1,0:T(8,128)(2,1)S(1)}, bf16[256,512]{1,0:T(8,128)(2,1)}, u32[]{:S(2)}) copy-start(bf16[256,512]{1,0:T(8,128)(2,1)} %param.10) | copy-start | bytes 786436
Sparse Core Ops, SparseCore 0:
  56.7 33.4 all-gather.4
  91.8 34.4 all-gather.2
  149.9 44.3 reduce-scatter.4
  212.4 62.2 reduce-scatter.6
where the time goes:
time: 292 us; the launch traced here: 288 us
  waiting for transfers between devices  83.4 us (29%)
  blocking collectives  78.4 us (27%)
  matrix products  66.9 us (23%)
  local copies, waits for them, and re-layouts  28.3 us (10%)
  between operations  14.5 us (5%)
  starting transfers between devices  11.3 us (4%)
  other arithmetic  5.26 us (2%)
    unnamed x5, waiting for transfers between devices  52.6 us
    all_to_all x1, blocking collectives, local(): lax.all_to_all(token_send, 'ep', split_axis=0, concat_axis=0, tiled=True)  33.1 us
    all_to_all x1, blocking collectives, local(): lax.all_to_all(output_send, 'ep', split_axis=0, concat_axis=0, tiled=True)  29 us
    reduce_scatter x1, waiting for transfers between devices, local(): lax.psum_scatter(slot_terms.reshape(senders, capacity, model_width).astyp...  23 us
    dot_general x1, matrix products, local(): lax.dot_general(output_rows, w_down, over_cols, preferred_element_type=jn...  12.6 us
    all_to_all x1, blocking collectives, local(): lax.all_to_all(mix_send, 'ep', split_axis=0, concat_axis=0, tiled=True)  9.84 us
    dot_general x1, matrix products, local(): gate_pre = jnp.dot(token_rows, w_gate, preferred_element_type=jnp.float32)  9.3 us
    dot_general x1, matrix products, local(): lax.dot_general(token_rows, up_back, over_rows, preferred_element_type=jn...  9.2 us
  transfers between devices with their start and end apart: 6, of which 3 were waited for; matrix products, arithmetic and copies ran while one was open for 19% of the time, Pallas kernels for 0%

commit v1 on v0

v1 whole, which is shorter than its diff:
```python
import math

import jax
import jax.numpy as jnp
from jax import lax
from jax.experimental import pallas as pl
from jax.experimental.pallas import tpu as pltpu
from jax.sharding import PartitionSpec as P

MESH = pl.DeviceIdType.MESH
LANES = 128
DIRECT_TOKENS = False


def remote(src, dst, send, recv, ep, tp):
    return pltpu.make_async_remote_copy(
        src_ref=src,
        dst_ref=dst,
        send_sem=send,
        recv_sem=recv,
        device_id=(ep, tp),
        device_id_type=MESH,
    )


def span(start, size):
    return pl.ds(pl.multiple_of(start * size, size), size)


def dispatch_kernel(senders, rows, capacity, col, direct):
    def body(tok_ref, cot_ref, mix_ref, tok_out, cot_out, mix_out, ep_send, ep_recv, y_send, y_recv,
             c_send, c_recv, m_send, m_recv, l_sem):
        me = lax.axis_index("ep")
        tp = lax.axis_index("tp")
        row = tp // 2
        core = tp % 2
        partner = row * 2 + (1 - core)

        def seat(step, side):
            return lax.rem(row + step + rows, rows) * 2 + side

        def piece(out, block, tp_col):
            return out.at[span(block, capacity), span(tp_col, col)]

        def source(array, dest, tp_col):
            if array == 0:
                return tok_ref.at[dest, :, span(tp_col // 2, col)] if direct else tok_ref.at[dest]
            return cot_ref.at[dest]

        items = [(1, 0), (0, 0)] + [(0, j) for j in range(1, rows) if direct]
        hops = [(a, j) for a in ((1,) if direct else (0, 1)) for j in range(1, rows)]
        outs = (tok_out, cot_out)

        def ep_copy(i, dest, block):
            array, which = items[i]
            return remote(source(array, dest, seat(which, core)), piece(outs[array], block, seat(which, core)),
                          ep_send.at[i, dest], ep_recv.at[i, block], dest, tp)

        def mix_copy(dest, block):
            return remote(mix_ref.at[dest], mix_out.at[block], m_send.at[dest], m_recv.at[block], dest, tp)

        def local_copy(i):
            array, which = items[i]
            return pltpu.make_async_copy(source(array, me, seat(which, core)),
                                         piece(outs[array], me, seat(which, core)), l_sem.at[i])

        local_mix = pltpu.make_async_copy(mix_ref.at[me], mix_out.at[me], l_sem.at[len(items)])

        def y_copy(array, step, block):
            place = piece(outs[array], block, tp)
            return remote(place, place, y_send.at[array, step, block], y_recv.at[array, step, block],
                          me, seat(step, core))

        def y_arrival(array, step, block):
            place = piece(outs[array], block, seat(-step, core))
            return remote(place, place, y_send.at[array, step, block], y_recv.at[array, step, block],
                          me, seat(step, core))

        def c_copy(array, step, block):
            place = piece(outs[array], block, seat(step, core))
            return remote(place, place, c_send.at[array, step + rows, block],
                          c_recv.at[array, step + rows, block], me, partner)

        def c_arrival(array, step, block):
            place = piece(outs[array], block, seat(step, 1 - core))
            return remote(place, place, c_send.at[array, step + rows, block],
                          c_recv.at[array, step + rows, block], me, partner)

        relays = items + [(array, -step) for array, step in hops]
        for i in range(len(items)):
            local_copy(i).start()
        local_mix.start()

        def send_all(k, carry):
            dest = lax.rem(me + k, senders)
            for i in range(len(items)):
                ep_copy(i, dest, me).start()
            mix_copy(dest, me).start()
            return carry

        lax.fori_loop(1, senders, send_all, 0)
        for i in range(len(items)):
            local_copy(i).wait()
        local_mix.wait()

        def spread(block):
            for array, step in hops:
                y_copy(array, step, block).start()
            for array, step in items:
                c_copy(array, step, block).start()

        def pass_on(block):
            for array, step in hops:
                y_arrival(array, step, block).wait_recv()
                c_copy(array, -step, block).start()

        spread(me)

        def relay(k, carry):
            block = lax.rem(me + senders - k, senders)
            for i in range(len(items)):
                ep_copy(i, block, block).wait_recv()
            spread(block)
            pass_on(lax.rem(me + senders - k + 1, senders))
            return carry

        lax.fori_loop(1, senders, relay, 0)
        pass_on(lax.rem(me + 1, senders))

        def finish(k, carry):
            block = lax.rem(me + k, senders)
            for array, step in relays:
                c_arrival(array, step, block).wait_recv()
                c_copy(array, step, block).wait_send()
            for array, step in hops:
                y_copy(array, step, block).wait_send()
            return carry

        lax.fori_loop(0, senders, finish, 0)

        def finish_ep(k, carry):
            block = lax.rem(me + k, senders)
            for i in range(len(items)):
                ep_copy(i, block, me).wait_send()
            mix_copy(block, me).wait_send()
            mix_copy(block, block).wait_recv()
            return carry

        lax.fori_loop(1, senders, finish_ep, 0)

    return body


def dispatch(tok_send, cot_send, mix_send, direct):
    senders, capacity, col = cot_send.shape
    width = col * lax.axis_size("tp")
    n_rows = lax.axis_size("tp") // 2
    vmem = pl.BlockSpec(memory_space=pltpu.VMEM)
    dma = pltpu.SemaphoreType.DMA
    rows = jax.ShapeDtypeStruct((senders * capacity, width), cot_send.dtype)
    return pl.pallas_call(
        dispatch_kernel(senders, n_rows, capacity, col, direct),
        out_shape=(rows, rows, jax.ShapeDtypeStruct(mix_send.shape, mix_send.dtype)),
        in_specs=[vmem] * 3,
        out_specs=[pl.BlockSpec(memory_space=pl.ANY)] * 2 + [vmem],
        scratch_shapes=[
            dma((2 + n_rows, senders)), dma((2 + n_rows, senders)),
            dma((2, n_rows, senders)), dma((2, n_rows, senders)),
            dma((2, 2 * n_rows, senders)), dma((2, 2 * n_rows, senders)),
            dma((senders,)), dma((senders,)),
            dma((3 + n_rows,)),
        ],
        compiler_params=pltpu.CompilerParams(has_side_effects=True, vmem_limit_bytes=24 << 20),
        name="dispatch",
    )(tok_send, cot_send, mix_send)


def combine_kernel(senders, rows, capacity, col):
    def body(terms, mix_ref, out, mix_out, c_buf, y_src, y_buf, fin, mix_got, mix_all,
             c_send, c_recv, y_send, y_recv, h_send, h_recv, m_send, m_recv, t_send, t_recv):
        me = lax.axis_index("ep")
        tp = lax.axis_index("tp")
        row = tp // 2
        core = tp % 2
        partner = row * 2 + (1 - core)

        def seat(step, side):
            return lax.rem(row + step + rows, rows) * 2 + side

        def c_copy(step, block):
            return remote(terms.at[block, :, span(seat(step, 1 - core), col)], c_buf.at[step, block],
                          c_send.at[step, block], c_recv.at[step, block], me, partner)

        def y_copy(step, block):
            return remote(y_src.at[step - 1, block], y_buf.at[step - 1, block],
                          y_send.at[step, block], y_recv.at[step, block], me, seat(step, core))

        def h_copy(dest, slot):
            return remote(fin.at[dest], out.at[slot], h_send.at[dest], h_recv.at[slot], dest, tp)

        def m_copy(dest, slot):
            return remote(mix_ref.at[dest], mix_got.at[slot], m_send.at[dest], m_recv.at[slot], dest, tp)

        def order(k):
            return lax.rem(me + k, senders)

        def start(k, carry):
            for step in list(range(1, rows)) + [0]:
                c_copy(step, order(k)).start()
            return carry

        lax.fori_loop(1, senders + 1, start, 0)

        def start_mix(k, carry):
            m_copy(order(k), me).start()
            return carry

        lax.fori_loop(1, senders, start_mix, 0)
        mix_got[me] = mix_ref[me]

        def first(block):
            for step in range(1, rows):
                c_copy(step, block).wait_recv()
                y_src[step - 1, block] = (
                    terms[block, :, span(seat(step, core), col)].astype(jnp.float32)
                    + c_buf[step, block].astype(jnp.float32)
                ).astype(y_src.dtype)
                y_copy(step, block).start()

        def total(block):
            c_copy(0, block).wait_recv()
            value = terms[block, :, span(tp, col)].astype(jnp.float32) + c_buf[0, block].astype(
                jnp.float32
            )
            for step in range(1, rows):
                y_copy(step, block).wait_recv()
                value = value + y_buf[step - 1, block].astype(jnp.float32)
            return value.astype(out.dtype)

        def second(block):
            fin[block] = total(block)
            h_copy(block, me).start()

        ahead = 2

        def lead(k, carry):
            first(order(k))
            return carry

        def steady(k, carry):
            first(order(k))
            second(order(k - ahead))
            return carry

        lax.fori_loop(1, 1 + ahead, lead, 0)
        lax.fori_loop(1 + ahead, senders + 1, steady, 0)

        def last(k, carry):
            second(order(k))
            return carry

        lax.fori_loop(senders + 1 - ahead, senders, last, 0)
        out[me] = total(me)

        def mix_arrive(k, carry):
            m_copy(order(k), order(k)).wait_recv()
            return carry

        lax.fori_loop(1, senders, mix_arrive, 0)
        mix_all[0] = mix_got[...]

        def t_copy(k):
            peer = lax.rem(tp + k, 2 * rows)
            return remote(mix_got, mix_all.at[k], t_send.at[k], t_recv.at[k], me, peer)

        for k in range(1, 2 * rows):
            t_copy(k).start()

        def finish(k, carry):
            block = order(k)
            for step in range(rows):
                c_copy(step, block).wait_send()
            for step in range(1, rows):
                y_copy(step, block).wait_send()
            return carry

        lax.fori_loop(0, senders, finish, 0)

        def finish_home(k, carry):
            block = order(k)
            h_copy(block, block).wait()
            m_copy(block, block).wait_send()
            return carry

        lax.fori_loop(1, senders, finish_home, 0)
        for k in range(1, 2 * rows):
            t_copy(k).wait()
        mix_out[...] = jnp.sum(mix_all[...], axis=0)

    return body


def combine(terms, mix_part):
    senders, capacity, width = terms.shape
    col = width // lax.axis_size("tp")
    n_rows = lax.axis_size("tp") // 2
    vmem = pl.BlockSpec(memory_space=pltpu.VMEM)
    dma = pltpu.SemaphoreType.DMA
    block = (senders, capacity, col)
    return pl.pallas_call(
        combine_kernel(senders, n_rows, capacity, col),
        out_shape=(
            jax.ShapeDtypeStruct(block, terms.dtype),
            jax.ShapeDtypeStruct(mix_part.shape, mix_part.dtype),
        ),
        in_specs=[vmem] * 2,
        out_specs=[vmem] * 2,
        scratch_shapes=[
            pltpu.VMEM((n_rows,) + block, terms.dtype),
            pltpu.VMEM((n_rows - 1,) + block, terms.dtype),
            pltpu.VMEM((n_rows - 1,) + block, terms.dtype),
            pltpu.VMEM(block, terms.dtype),
            pltpu.VMEM(mix_part.shape, mix_part.dtype),
            pltpu.VMEM((2 * n_rows,) + mix_part.shape, mix_part.dtype),
            dma((n_rows, senders)), dma((n_rows, senders)),
            dma((n_rows, senders)), dma((n_rows, senders)),
            dma((senders,)), dma((senders,)),
            dma((senders,)), dma((senders,)),
            dma((2 * n_rows,)), dma((2 * n_rows,)),
        ],
        compiler_params=pltpu.CompilerParams(has_side_effects=True, vmem_limit_bytes=32 << 20),
        name="combine",
    )(terms, mix_part)


def router_sum(terms):
    senders = terms.shape[0]

    def body(src, out, got, send, recv):
        me = lax.axis_index("ep")
        tp = lax.axis_index("tp")

        def copy(dest, slot):
            return remote(src.at[dest], got.at[slot], send.at[dest], recv.at[slot], dest, tp)

        def start(k, carry):
            copy(lax.rem(me + k, senders), me).start()
            return carry

        lax.fori_loop(1, senders, start, 0)
        got[me] = src[me]

        def wait(k, carry):
            block = lax.rem(me + k, senders)
            copy(block, block).wait()
            return carry

        lax.fori_loop(1, senders, wait, 0)
        out[...] = jnp.sum(got[...], axis=0)

    vmem = pl.BlockSpec(memory_space=pltpu.VMEM)
    dma = pltpu.SemaphoreType.DMA
    return pl.pallas_call(
        body,
        out_shape=jax.ShapeDtypeStruct(terms.shape[1:], terms.dtype),
        in_specs=[vmem],
        out_specs=vmem,
        scratch_shapes=[pltpu.VMEM(terms.shape, terms.dtype), dma((senders,)), dma((senders,))],
        compiler_params=pltpu.CompilerParams(has_side_effects=True, vmem_limit_bytes=8 << 20),
        name="router_sum",
    )(terms)


def slot_places(flat_routes, experts, capacity):
    entries = flat_routes.shape[0]
    onehot = flat_routes[:, None] == jnp.arange(experts, dtype=jnp.int32)[None, :]
    index = jnp.arange(entries, dtype=jnp.int32)
    before = (index[None, :] < index[:, None]).astype(jnp.bfloat16)
    earlier = jnp.dot(before, onehot.astype(jnp.bfloat16), preferred_element_type=jnp.float32)
    rank = jnp.sum(jnp.where(onehot, earlier, 0.0), axis=1).astype(jnp.int32)
    return flat_routes * capacity + rank


def pad_lanes(rows):
    return jnp.pad(rows[:, None, :], ((0, 0), (0, 7), (0, LANES - rows.shape[1])))


def local(tokens, routes, router_matrix, cotangent, gate_proj, up_proj, down_proj):
    ep_size = lax.axis_size("ep")
    tp_size = lax.axis_size("tp")
    tp_index = lax.axis_index("tp")
    home_rows, model_width = tokens.shape
    top_count = routes.shape[1]
    experts = router_matrix.shape[1]
    capacity = home_rows * top_count * 2 // experts
    col_width = model_width // tp_size
    places = slot_places(routes.reshape(-1), experts, capacity).reshape(home_rows, top_count)
    slot_ids = jnp.arange(experts * capacity, dtype=jnp.int32)
    hits = slot_ids[:, None, None] == places.T[None, :, :]
    pick = jnp.any(hits, axis=1).astype(jnp.bfloat16)
    logits = jnp.dot(tokens, router_matrix, preferred_element_type=jnp.float32)
    picked = routes[:, :, None] == jnp.arange(experts, dtype=jnp.int32)[None, None, :]
    chosen = jnp.sum(jnp.where(picked, logits[:, None, :], 0.0), axis=2)
    mixing = jax.nn.sigmoid(chosen - chosen[:, ::-1])
    mix_send = jnp.sum(jnp.where(hits, mixing.T[None, :, :], 0.0), axis=(1, 2))
    mix_send = pad_lanes(mix_send.reshape(experts, capacity))
    if DIRECT_TOKENS:
        token_cols = lax.dynamic_slice_in_dim(
            tokens.reshape(home_rows, tp_size // 2, 2, col_width), tp_index % 2, 1, 2
        ).reshape(home_rows, model_width // 2)
    else:
        token_cols = lax.dynamic_slice_in_dim(tokens, tp_index * col_width, col_width, 1)
    token_send = jnp.dot(pick, token_cols, preferred_element_type=jnp.float32).astype(
        jnp.bfloat16
    ).reshape(experts, capacity, -1)
    output_send = jnp.dot(pick, cotangent, preferred_element_type=jnp.float32).astype(
        jnp.bfloat16
    ).reshape(experts, capacity, col_width)
    token_rows, output_rows, mix_in = dispatch(token_send, output_send, mix_send, DIRECT_TOKENS)
    senders = ep_size
    slots = senders * capacity
    mix_value = mix_in[:, 0, :capacity].reshape(slots).astype(jnp.bfloat16).astype(jnp.float32)
    w_gate = gate_proj[0]
    w_up = up_proj[0]
    w_down = down_proj[0]
    over_rows = (((0,), (0,)), ((), ()))
    over_cols = (((1,), (1,)), ((), ()))
    gate_pre = jnp.dot(token_rows, w_gate, preferred_element_type=jnp.float32)
    up_pre = jnp.dot(token_rows, w_up, preferred_element_type=jnp.float32)
    gate_sig = jax.nn.sigmoid(gate_pre)
    active = gate_pre * gate_sig
    hidden = (active * up_pre).astype(jnp.bfloat16)
    back_hidden = lax.dot_general(
        output_rows, w_down, over_cols, preferred_element_type=jnp.float32
    )
    mix_part = jnp.sum(hidden.astype(jnp.float32) * back_hidden, axis=1)
    scaled = mix_value[:, None] * back_hidden
    gate_back = (scaled * up_pre * gate_sig * (1.0 + gate_pre * (1.0 - gate_sig))).astype(
        jnp.bfloat16
    )
    up_back = (scaled * active).astype(jnp.bfloat16)
    out_scaled = (mix_value[:, None] * output_rows).astype(jnp.bfloat16)
    slot_terms = lax.dot_general(gate_back, w_gate, over_cols, preferred_element_type=jnp.float32)
    slot_terms = slot_terms + lax.dot_general(
        up_back, w_up, over_cols, preferred_element_type=jnp.float32
    )
    gate_grad = lax.dot_general(
        token_rows, gate_back, over_rows, preferred_element_type=jnp.float32
    ).astype(jnp.bfloat16)[None]
    up_grad = lax.dot_general(
        token_rows, up_back, over_rows, preferred_element_type=jnp.float32
    ).astype(jnp.bfloat16)[None]
    down_grad = lax.dot_general(
        hidden, out_scaled, over_rows, preferred_element_type=jnp.float32
    ).astype(jnp.bfloat16)[None]
    back_rows, back_mix = combine(
        slot_terms.astype(jnp.bfloat16).reshape(senders, capacity, model_width),
        pad_lanes(mix_part.reshape(senders, capacity)),
    )
    back_flat = back_rows.reshape(experts * capacity, col_width)
    over_slots = (((0,), (0,)), ((), ()))
    token_part = lax.dot_general(pick, back_flat, over_slots, preferred_element_type=jnp.float32)
    mix_flat = back_mix[:, 0, :capacity].reshape(experts * capacity)
    mixing_grad = jnp.sum(jnp.where(hits, mix_flat[:, None, None], 0.0), axis=0).T
    pairwise = mixing[:, 0] * mixing[:, 1]
    logit_grad = pairwise[:, None] * (mixing_grad - mixing_grad[:, ::-1])
    route_grad = jnp.sum(jnp.where(picked, logit_grad[:, :, None], 0.0), axis=1)
    router_cols = lax.dynamic_slice_in_dim(
        router_matrix, tp_index * col_width, col_width, 0
    ).astype(jnp.float32)
    router_path = jnp.dot(route_grad, router_cols.T, precision=lax.Precision.HIGHEST)
    token_grad = (token_part + router_path).astype(jnp.bfloat16)
    row_share = model_width // (ep_size * tp_size)
    feature_share = lax.dynamic_slice_in_dim(
        tokens.reshape(home_rows, ep_size, tp_size, row_share), tp_index, 1, 2
    )
    feature_share = feature_share.reshape(home_rows, ep_size * row_share).astype(jnp.float32)
    norm_scale = 1.0 / math.sqrt(home_rows * ep_size)
    router_terms = (
        jnp.dot(route_grad.T, feature_share, precision=lax.Precision.HIGHEST) * norm_scale
    )
    router_terms = jnp.swapaxes(router_terms.reshape(experts, ep_size, row_share), 0, 1)
    router_terms = jnp.pad(router_terms, ((0, 0), (0, 0), (0, LANES - row_share)))
    router_grad = router_sum(router_terms)[:, :row_share].T
    return (token_grad, mixing_grad, router_grad, gate_grad, up_grad, down_grad)


def solution(mesh):
    return jax.shard_map(
        local,
        mesh=mesh,
        in_specs=(
            P("ep", None),
            P("ep", None),
            P(),
            P("ep", "tp"),
            P("ep", None, "tp"),
            P("ep", None, "tp"),
            P("ep", "tp", None),
        ),
        out_specs=(
            P("ep", "tp"),
            P("ep", None),
            P(("ep", "tp"), None),
            P("ep", None, "tp"),
            P("ep", None, "tp"),
            P("ep", "tp", None),
        ),
        check_vma=False,
    )
```

time: 292 us -> 196 us (0.67); the launches traced: 288 us -> 196 us
  Pallas kernels: 0 us -> 132 us
  waiting for transfers between devices: 83.4 us -> 0 us
  blocking collectives: 78.4 us -> 0 us
  local copies, waits for them, and re-layouts: 28.3 us -> 4.46 us
  between operations: 14.5 us -> 0.95 us
  starting transfers between devices: 11.3 us -> 0 us
  matrix products: 66.9 us -> 56.4 us
  other arithmetic: 5.26 us -> 1.78 us
    pallas_call x0 -> x3, Pallas kernels: none -> 132 us  [the longest x1 74.1 us: dispatch(): pl.pallas_call(dispatch_kernel(senders, n_rows, capacity, col, direct), o...]
    all_to_all x3 -> x0, blocking collectives: 71.9 us -> none  [the longest x1 33.1 us: local(): lax.all_to_all(token_send, 'ep', split_axis=0, concat_axis=0, tiled=True)]
    unnamed x5 -> x0, waiting for transfers between devices: 52.6 us -> none
    reduce_scatter x1 -> x0, waiting for transfers between devices: 23 us -> none  [local(): lax.psum_scatter(slot_terms.reshape(senders, capacity, model_width).astyp...]
    gather x5 -> x0, local copies, waits for them, and re-layouts: 19 us -> none  [the longest x1 6.8 us: local(): mixing.reshape(-1)[entry_src]]
    all_to_all x2 -> x0, starting transfers between devices: 11.2 us -> none  [the longest x1 5.66 us: local(): lax.all_to_all(mix_total, 'ep', split_axis=0, concat_axis=0, tiled=True)]
    all_gather x2 -> x0, waiting for transfers between devices: 7.76 us -> none  [the longest x1 7.75 us: local(): lax.all_gather(output_part_in, 'tp', axis=2, tiled=True)]
    psum x1 -> x0, blocking collectives: 6.49 us -> none  [local(): mix_total = lax.psum(mix_part.reshape(senders, capacity), 'tp')]
  transfers between devices with their start and end apart: 6 -> 0, of which waited for: 3 -> 0; matrix products, arithmetic and copies ran while one was open for 19% -> 0% of each run, Pallas kernels for 0% -> 0%
where the time goes in v1:
time: 196 us
  Pallas kernels  132 us (67%)
  matrix products  56.4 us (29%)
  local copies, waits for them, and re-layouts  4.46 us (2%)
    pallas_call x1, Pallas kernels, dispatch(): pl.pallas_call(dispatch_kernel(senders, n_rows, capacity, col, direct), o...  74.1 us
    pallas_call x1, Pallas kernels, combine(): pl.pallas_call(combine_kernel(senders, n_rows, capacity, col), out_shape=...  46.1 us
    pallas_call x1, Pallas kernels, router_sum(): pl.pallas_call(body, out_shape=jax.ShapeDtypeStruct(terms.shape[1:], term...  12.1 us
    dot_general x1, matrix products, local(): lax.dot_general(token_rows, up_back, over_rows, preferred_element_type=jn...  9.34 us
    dot_general x1, matrix products, local(): lax.dot_general(output_rows, w_down, over_cols, preferred_element_type=jn...  7.78 us
    dot_general x1, matrix products, local(): lax.dot_general(token_rows, gate_back, over_rows, preferred_element_type=...  6.02 us
    dot_general x1, matrix products, local(): gate_pre = jnp.dot(token_rows, w_gate, preferred_element_type=jnp.float32)  5.97 us
    dot_general x1, matrix products, local(): up_pre = jnp.dot(token_rows, w_up, preferred_element_type=jnp.float32)  5.85 us

profile of v1, /device:TPU:0, one launch (start us, length us, event | category | flops | bytes accessed | tf_op | source)
XLA Modules:
  0.0 195.9 jit_solution(12783025124686447565)
XLA Ops:
  0.6 0.0 copy-start
  0.6 0.0 copy-start.4
  0.7 0.9 copy.31
  1.5 0.1 eq.42
  1.7 0.3 fusion.14
  2.0 0.1 convert_element_type.73
  2.1 0.1 copy.32
  2.2 0.7 add_bitcast_fusion
  2.9 0.4 fusion.12
  3.3 1.4 convolution_convert_fusion.1
  4.7 1.6 fusion.22
  6.3 0.0 copy-done.4
  6.3 0.1 rev.6
  6.4 0.0 copy-start.7
  6.4 0.3 select_reduce_fusion.1
  6.7 0.0 copy-done
  6.8 0.4 convolution_convert_fusion
  7.2 74.1 %dispatch.1 = (bf16[1024,2048]{1,0:T(8,128)(2,1)S(1)}, bf16[1024,2048]{1,0:T(8,128)(2,1)S(1)}, f32[8,8,128]{2,1,0:T(8,128)S(1)}) custom-call(bf16[8,128,512]{2,1,0:T(8,128)(2,1)S(1)} %bitcast.63, bf16[8,128,512]{2,1,0:T(8,128)(2,1)S(1)} %bitcast.64, f32[8,8,128]{2,1,0:T(8,128)S(1)} %pad.11.mix_ref), custom_call_target="tpu_custom_call" | custom-call | tf_op jit(solution)/shard_map/dispatch/pallas_call | solution.py:161
  81.3 0.0 copy-start.1
  81.3 0.0 copy-done.7
  81.3 0.0 copy-start.8
  81.3 6.0 %fusion.4 = f32[1024,896]{0,1:T(8,128)} fusion(bf16[1024,2048]{1,0:T(8,128)(2,1)S(1)} %get-tuple-element.13, bf16[1,2048,896]{2,1,0:T(8,128)(2,1)S(1)} %copy-done.7), kind=kOutput, calls=%fused_computation.6 | convolution fusion | flops 3758096384 | bytes 11534336 | tf_op jit(solution)/shard_map/dot_general | solution.py:428
  87.3 0.0 copy-done.1
  87.3 0.0 copy-done.8
  87.3 0.0 copy-start.6
  87.3 5.8 %fusion.7 = f32[1024,896]{0,1:T(8,128)} fusion(bf16[1024,2048]{1,0:T(8,128)(2,1)S(1)} %get-tuple-element.13, bf16[1,2048,896]{2,1,0:T(8,128)(2,1)S(1)} %copy-done.8), kind=kOutput, calls=%fused_computation.9 | convolution fusion | flops 3758096384 | bytes 11534336 | tf_op jit(solution)/shard_map/dot_general | solution.py:429
  93.2 0.0 copy-done.6
  93.2 7.8 %multiply_reduce_fusion = (f32[1024]{0:T(1024)S(1)}, bf16[1024,896]{0,1:T(8,128)(2,1)S(1)}, bf16[1024,896]{0,1:T(8,128)(2,1)S(1)}, bf16[1024,896]{0,1:T(8,128)(2,1)S(1)}) fusion(f32[1024,896]{0,1:T(8,128)} %fusion.7, f32[1024,896]{0,1:T(8,128)} %fusion.4, f32[1024]{0:T(1024)S(1)} %bitcast.76, bf16[1024,2048]{1,0:T(8,128)(2,1)S(1)} %get-tuple-element.12, ...), kind=kOutput, calls=%fused_computation.16 | convolution fusion | flops 3775527936 | bytes 20717568 | tf_op jit(solution)/shard_map/dot_general | solution.py:433
  101.0 0.0 copy-start.9
  101.0 0.0 copy-start.11
  101.0 5.8 %convert_bitcast_fusion = bf16[1,896,2048]{2,1,0:T(8,128)(2,1)} fusion(bf16[1024,896]{0,1:T(8,128)(2,1)S(1)} %get-tuple-element.17, bf16[1024,2048]{1,0:T(8,128)(2,1)S(1)} %get-tuple-element.12, f32[1024]{0:T(1024)S(1)} %bitcast.77), kind=kOutput, calls=%fused_computation.13 | convolution fusion | flops 3766222848 | bytes 9703424 | tf_op jit(solution)/shard_map/dot_general | solution.py:453
  106.8 0.0 copy-done.9
  106.8 4.6 %fusion.2 = f32[1024,2048]{1,0:T(8,128)S(1)} fusion(bf16[1024,896]{0,1:T(8,128)(2,1)S(1)} %get-tuple-element.18, bf16[1,2048,896]{2,1,0:T(8,128)(2,1)S(1)} %copy-done.7), kind=kOutput, calls=%fused_computation.4 | convolution fusion | flops 3758096384 | bytes 13893632 | tf_op jit(solution)/shard_map/dot_general | solution.py:443
  111.3 0.0 copy-done.11
  111.4 4.8 %add_convert_fusion = bf16[1024,2048]{1,0:T(8,128)(2,1)S(1)} fusion(f32[1024,2048]{1,0:T(8,128)S(1)} %fusion.2, bf16[1024,896]{0,1:T(8,128)(2,1)S(1)} %get-tuple-element.19, bf16[1,2048,896]{2,1,0:T(8,128)(2,1)S(1)} %copy-done.8), kind=kOutput, calls=%fused_computation.1 | convolution fusion | flops 3762290688 | bytes 18087936 | tf_op jit(solution)/shard_map/dot_general | solution.py:444
  116.2 0.0 copy-start.3
  116.2 46.1 %combine.1 = (bf16[8,128,512]{2,1,0:T(8,128)(2,1)S(1)}, f32[8,8,128]{2,1,0:T(8,128)S(1)}) custom-call(bf16[8,128,2048]{2,1,0:T(8,128)(2,1)S(1)} %bitcast.62, f32[8,8,128]{2,1,0:T(8,128)S(1)} %pad.12.mix_ref), custom_call_target="tpu_custom_call" | custom-call | tf_op jit(solution)/shard_map/combine/pallas_call | solution.py:310
  162.3 0.3 select_reduce_fusion
  162.7 0.0 copy-start.5
  162.7 0.1 rev.7
  162.8 0.0 copy-done.3
  162.8 1.3 copy.33
  164.1 1.0 constant_dynamic-slice_fusion
  165.1 0.3 convolution_multiply_fusion
  165.4 0.1 reshape.59
  165.5 12.1 %router_sum.1 = f32[8,128]{1,0:T(8,128)S(1)} custom-call(f32[8,8,128]{2,1,0:T(8,128)S(1)} %pad.13.src), custom_call_target="tpu_custom_call" | custom-call | tf_op jit(solution)/shard_map/router_sum/pallas_call | solution.py:363
  177.7 0.6 slice_bitcast_fusion
  178.2 0.0 copy-start.2
  178.3 0.0 copy-start.10
  178.3 9.3 %convert_bitcast_fusion.1 = bf16[1,2048,896]{2,1,0:T(8,128)(2,1)} fusion(bf16[1024,2048]{1,0:T(8,128)(2,1)} %copy-done.1, bf16[1024,896]{0,1:T(8,128)(2,1)} %copy-done.11), kind=kOutput, calls=%fused_computation.14 | convolution fusion | flops 3759931392 | bytes 9699328 | tf_op jit(solution)/shard_map/dot_general | solution.py:450
  187.6 0.0 copy-done.5
  187.6 0.0 copy-done.2
  187.6 0.0 copy-done.10
  187.6 6.0 %convert_bitcast_fusion.2 = bf16[1,2048,896]{2,1,0:T(8,128)(2,1)} fusion(bf16[1024,2048]{1,0:T(8,128)(2,1)S(1)} %copy-done.2, bf16[1024,896]{0,1:T(8,128)(2,1)S(1)} %copy-done.10), kind=kOutput, calls=%fused_computation.15 | convolution fusion | flops 3759931392 | bytes 9699328 | tf_op jit(solution)/shard_map/dot_general | solution.py:447
  193.6 1.1 fusion.16
  194.7 1.2 fusion.13
  (12 shorter events, 0.1 us)
Async XLA Ops:
  0.6 6.1 %copy-start = (bf16[256,512]{1,0:T(8,128)(2,1)S(1)}, bf16[256,512]{1,0:T(8,128)(2,1)}, u32[]{:S(2)}) copy-start(bf16[256,512]{1,0:T(8,128)(2,1)} %param.10) | copy-start | bytes 786436
  0.6 5.6 %copy-start.4 = (s32[256,2]{0,1:T(2,128)S(1)}, s32[256,2]{0,1:T(2,128)}, u32[]{:S(2)}) copy-start(s32[256,2]{0,1:T(2,128)} %param.8) | copy-start | bytes 6148
  6.4 74.9 %copy-start.7 = (bf16[1,2048,896]{2,1,0:T(8,128)(2,1)S(1)}, bf16[1,2048,896]{2,1,0:T(8,128)(2,1)}, u32[]{:S(2)}) copy-start(bf16[1,2048,896]{2,1,0:T(8,128)(2,1)} %param.11) | copy-start | bytes 11010052
  81.3 6.0 %copy-start.1 = (bf16[1024,2048]{1,0:T(8,128)(2,1)}, bf16[1024,2048]{1,0:T(8,128)(2,1)S(1)}, u32[]{:S(2)}) copy-start(bf16[1024,2048]{1,0:T(8,128)(2,1)S(1)} %get-tuple-element.13) | copy-start | bytes 12582916
  81.3 6.0 %copy-start.8 = (bf16[1,2048,896]{2,1,0:T(8,128)(2,1)S(1)}, bf16[1,2048,896]{2,1,0:T(8,128)(2,1)}, u32[]{:S(2)}) copy-start(bf16[1,2048,896]{2,1,0:T(8,128)(2,1)} %param.12) | copy-start | bytes 11010052
  87.3 5.9 %copy-start.6 = (bf16[1,896,2048]{2,1,0:T(8,128)(2,1)S(1)}, bf16[1,896,2048]{2,1,0:T(8,128)(2,1)}, u32[]{:S(2)}) copy-start(bf16[1,896,2048]{2,1,0:T(8,128)(2,1)} %param.13) | copy-start | bytes 11010052
  101.0 5.8 %copy-start.9 = (bf16[1024,896]{0,1:T(8,128)(2,1)}, bf16[1024,896]{0,1:T(8,128)(2,1)S(1)}, u32[]{:S(2)}) copy-start(bf16[1024,896]{0,1:T(8,128)(2,1)S(1)} %get-tuple-element.18) | copy-start | bytes 5505028
  101.0 10.4 %copy-start.11 = (bf16[1024,896]{0,1:T(8,128)(2,1)}, bf16[1024,896]{0,1:T(8,128)(2,1)S(1)}, u32[]{:S(2)}) copy-start(bf16[1024,896]{0,1:T(8,128)(2,1)S(1)} %get-tuple-element.19) | copy-start | bytes 5505028
  116.2 46.7 %copy-start.3 = (bf16[256,2048]{1,0:T(8,128)(2,1)S(1)}, bf16[256,2048]{1,0:T(8,128)(2,1)}, u32[]{:S(2)}) copy-start(bf16[256,2048]{1,0:T(8,128)(2,1)} %param.7) | copy-start | bytes 3145732
  162.7 24.9 %copy-start.5 = (f32[2,256]{1,0:T(2,128)}, f32[2,256]{1,0:T(2,128)S(1)}, u32[]{:S(2)}) copy-start(f32[2,256]{1,0:T(2,128)S(1)} %select_reduce_fusion) | copy-start | bytes 6148
  178.2 9.3 %copy-start.2 = (bf16[1024,2048]{1,0:T(8,128)(2,1)S(1)}, bf16[1024,2048]{1,0:T(8,128)(2,1)}, u32[]{:S(2)}) copy-start(bf16[1024,2048]{1,0:T(8,128)(2,1)} %copy-done.1) | copy-start | bytes 12582916
  178.3 9.3 %copy-start.10 = (bf16[1024,896]{0,1:T(8,128)(2,1)S(1)}, bf16[1024,896]{0,1:T(8,128)(2,1)}, u32[]{:S(2)}) copy-start(bf16[1024,896]{0,1:T(8,128)(2,1)} %copy-done.9) | copy-start | bytes 5505028

commit v2 on v1

--- a/solution.py
+++ b/solution.py
@@ -9,7 +9,6 @@
 
 MESH = pl.DeviceIdType.MESH
 LANES = 128
-DIRECT_TOKENS = False
 
 
 def remote(src, dst, send, recv, ep, tp):
@@ -23,11 +22,23 @@
     )
 
 
+def pair(me, k, size):
+    if size & (size - 1):
+        return lax.rem(me + k, size)
+    return sum((me // bit + k // bit) % 2 * bit for bit in (1 << b for b in range(size.bit_length() - 1)))
+
+
+def came(me, k, size):
+    if size & (size - 1):
+        return lax.rem(me + size - k, size)
+    return pair(me, k, size)
+
+
 def span(start, size):
     return pl.ds(pl.multiple_of(start * size, size), size)
 
 
-def dispatch_kernel(senders, rows, capacity, col, direct):
+def dispatch_kernel(senders, rows, capacity, col):
     def body(tok_ref, cot_ref, mix_ref, tok_out, cot_out, mix_out, ep_send, ep_recv, y_send, y_recv,
              c_send, c_recv, m_send, m_recv, l_sem):
         me = lax.axis_index("ep")
@@ -44,15 +55,18 @@
 
         def source(array, dest, tp_col):
             if array == 0:
-                return tok_ref.at[dest, :, span(tp_col // 2, col)] if direct else tok_ref.at[dest]
+                return tok_ref.at[dest, :, span(tp_col // 2, col)]
             return cot_ref.at[dest]
 
-        items = [(1, 0), (0, 0)] + [(0, j) for j in range(1, rows) if direct]
-        hops = [(a, j) for a in ((1,) if direct else (0, 1)) for j in range(1, rows)]
+        far = [(1, 0), (0, 0)]
+        near = far + [(0, j) for j in range(1, rows)]
+        far_hops = [(a, j) for j in range(1, rows) for a in (1, 0)]
+        near_hops = [(1, j) for j in range(1, rows)]
+        half = max(senders // 2, 1)
         outs = (tok_out, cot_out)
 
         def ep_copy(i, dest, block):
-            array, which = items[i]
+            array, which = near[i]
             return remote(source(array, dest, seat(which, core)), piece(outs[array], block, seat(which, core)),
                           ep_send.at[i, dest], ep_recv.at[i, block], dest, tp)
 
@@ -60,11 +74,11 @@
             return remote(mix_ref.at[dest], mix_out.at[block], m_send.at[dest], m_recv.at[block], dest, tp)
 
         def local_copy(i):
-            array, which = items[i]
+            array, which = near[i]
             return pltpu.make_async_copy(source(array, me, seat(which, core)),
                                          piece(outs[array], me, seat(which, core)), l_sem.at[i])
 
-        local_mix = pltpu.make_async_copy(mix_ref.at[me], mix_out.at[me], l_sem.at[len(items)])
+        local_mix = pltpu.make_async_copy(mix_ref.at[me], mix_out.at[me], l_sem.at[len(near)])
 
         def y_copy(array, step, block):
             place = piece(outs[array], block, tp)
@@ -86,72 +100,90 @@
             return remote(place, place, c_send.at[array, step + rows, block],
                           c_recv.at[array, step + rows, block], me, partner)
 
-        relays = items + [(array, -step) for array, step in hops]
-        for i in range(len(items)):
+        relays = far + [(array, -step) for array, step in far_hops]
+        near_relays = near + [(array, -step) for array, step in near_hops]
+
+        def send_all(count):
+            def step(k, carry):
+                dest = pair(me, k, senders)
+                for i in range(count):
+                    ep_copy(i, dest, me).start()
+                mix_copy(dest, me).start()
+                return carry
+
+            return step
+
+        lax.fori_loop(1, half, send_all(len(near)), 0)
+        lax.fori_loop(half, senders, send_all(len(far)), 0)
+        for i in range(len(near)):
             local_copy(i).start()
         local_mix.start()
-
-        def send_all(k, carry):
-            dest = lax.rem(me + k, senders)
-            for i in range(len(items)):
-                ep_copy(i, dest, me).start()
-            mix_copy(dest, me).start()
-            return carry
-
-        lax.fori_loop(1, senders, send_all, 0)
-        for i in range(len(items)):
+        for i in range(len(near)):
             local_copy(i).wait()
         local_mix.wait()
 
-        def spread(block):
+        def spread(block, items, hops):
             for array, step in hops:
                 y_copy(array, step, block).start()
             for array, step in items:
                 c_copy(array, step, block).start()
 
-        def pass_on(block):
+        def pass_on(block, hops):
             for array, step in hops:
                 y_arrival(array, step, block).wait_recv()
                 c_copy(array, -step, block).start()
 
-        spread(me)
-
-        def relay(k, carry):
-            block = lax.rem(me + senders - k, senders)
-            for i in range(len(items)):
-                ep_copy(i, block, block).wait_recv()
-            spread(block)
-            pass_on(lax.rem(me + senders - k + 1, senders))
-            return carry
-
-        lax.fori_loop(1, senders, relay, 0)
-        pass_on(lax.rem(me + 1, senders))
-
-        def finish(k, carry):
-            block = lax.rem(me + k, senders)
-            for array, step in relays:
-                c_arrival(array, step, block).wait_recv()
-                c_copy(array, step, block).wait_send()
-            for array, step in hops:
-                y_copy(array, step, block).wait_send()
-            return carry
-
-        lax.fori_loop(0, senders, finish, 0)
-
-        def finish_ep(k, carry):
-            block = lax.rem(me + k, senders)
-            for i in range(len(items)):
-                ep_copy(i, block, me).wait_send()
-            mix_copy(block, me).wait_send()
-            mix_copy(block, block).wait_recv()
-            return carry
-
-        lax.fori_loop(1, senders, finish_ep, 0)
+        spread(me, near, near_hops)
+
+        def relay(items, hops, past_hops):
+            def step(k, carry):
+                block = came(me, k, senders)
+                for i in range(len(items)):
+                    ep_copy(i, block, block).wait_recv()
+                spread(block, items, hops)
+                pass_on(came(me, k - 1, senders), past_hops)
+                return carry
+
+            return step
+
+        lax.fori_loop(1, half, relay(near, near_hops, near_hops), 0)
+        lax.fori_loop(half, min(half + 1, senders), relay(far, far_hops, near_hops), 0)
+        lax.fori_loop(half + 1, senders, relay(far, far_hops, far_hops), 0)
+        pass_on(came(me, senders - 1, senders), far_hops if senders > 1 else near_hops)
+
+        def finish(through, hops):
+            def step(k, carry):
+                block = came(me, k, senders)
+                for array, step in through:
+                    c_arrival(array, step, block).wait_recv()
+                    c_copy(array, step, block).wait_send()
+                for array, step in hops:
+                    y_copy(array, step, block).wait_send()
+                return carry
+
+            return step
+
+        lax.fori_loop(0, half, finish(near_relays, near_hops), 0)
+        lax.fori_loop(half, senders, finish(relays, far_hops), 0)
+
+        def finish_ep(count):
+            def step(k, carry):
+                dest, block = pair(me, k, senders), came(me, k, senders)
+                for i in range(count):
+                    ep_copy(i, dest, me).wait_send()
+                mix_copy(dest, me).wait_send()
+                mix_copy(block, block).wait_recv()
+                return carry
+
+            return step
+
+        lax.fori_loop(1, half, finish_ep(len(near)), 0)
+        lax.fori_loop(half, senders, finish_ep(len(far)), 0)
 
     return body
 
 
-def dispatch(tok_send, cot_send, mix_send, direct):
+def dispatch(tok_send, cot_send, mix_send):
     senders, capacity, col = cot_send.shape
     width = col * lax.axis_size("tp")
     n_rows = lax.axis_size("tp") // 2
@@ -159,7 +191,7 @@
     dma = pltpu.SemaphoreType.DMA
     rows = jax.ShapeDtypeStruct((senders * capacity, width), cot_send.dtype)
     return pl.pallas_call(
-        dispatch_kernel(senders, n_rows, capacity, col, direct),
+        dispatch_kernel(senders, n_rows, capacity, col),
         out_shape=(rows, rows, jax.ShapeDtypeStruct(mix_send.shape, mix_send.dtype)),
         in_specs=[vmem] * 3,
         out_specs=[pl.BlockSpec(memory_space=pl.ANY)] * 2 + [vmem],
@@ -202,7 +234,7 @@
             return remote(mix_ref.at[dest], mix_got.at[slot], m_send.at[dest], m_recv.at[slot], dest, tp)
 
         def order(k):
-            return lax.rem(me + k, senders)
+            return pair(me, senders - k, senders)
 
         def start(k, carry):
             for step in list(range(1, rows)) + [0]:
@@ -404,19 +436,16 @@
     mixing = jax.nn.sigmoid(chosen - chosen[:, ::-1])
     mix_send = jnp.sum(jnp.where(hits, mixing.T[None, :, :], 0.0), axis=(1, 2))
     mix_send = pad_lanes(mix_send.reshape(experts, capacity))
-    if DIRECT_TOKENS:
-        token_cols = lax.dynamic_slice_in_dim(
-            tokens.reshape(home_rows, tp_size // 2, 2, col_width), tp_index % 2, 1, 2
-        ).reshape(home_rows, model_width // 2)
-    else:
-        token_cols = lax.dynamic_slice_in_dim(tokens, tp_index * col_width, col_width, 1)
+    token_cols = lax.dynamic_slice_in_dim(
+        tokens.reshape(home_rows, tp_size // 2, 2, col_width), tp_index % 2, 1, 2
+    ).reshape(home_rows, model_width // 2)
     token_send = jnp.dot(pick, token_cols, preferred_element_type=jnp.float32).astype(
         jnp.bfloat16
     ).reshape(experts, capacity, -1)
     output_send = jnp.dot(pick, cotangent, preferred_element_type=jnp.float32).astype(
         jnp.bfloat16
     ).reshape(experts, capacity, col_width)
-    token_rows, output_rows, mix_in = dispatch(token_send, output_send, mix_send, DIRECT_TOKENS)
+    token_rows, output_rows, mix_in = dispatch(token_send, output_send, mix_send)
     senders = ep_size
     slots = senders * capacity
     mix_value = mix_in[:, 0, :capacity].reshape(slots).astype(jnp.bfloat16).astype(jnp.float32)

time: 196 us -> 179 us (0.913)
  Pallas kernels: 132 us -> 117 us
    pallas_call x1, Pallas kernels: 46.1 us -> 37 us  [combine(): pl.pallas_call(combine_kernel(senders, n_rows, capacity, col), out_shape=...]
    pallas_call x1, Pallas kernels: 74.1 us -> 70 us  [dispatch(): pl.pallas_call(dispatch_kernel(senders, n_rows, capacity, col), out_shape...]
    dot_general x1, matrix products: 9.34 us -> 6.02 us  [local(): lax.dot_general(token_rows, up_back, over_rows, preferred_element_type=jn...]
    pallas_call x1, Pallas kernels: 12.1 us -> 9.63 us  [router_sum(): pl.pallas_call(body, out_shape=jax.ShapeDtypeStruct(terms.shape[1:], term...]
    dot_general x1, matrix products: 5.79 us -> 7.82 us  [local(): lax.dot_general(hidden, out_scaled, over_rows, preferred_element_type=jnp...]
where the time goes in v2:
time: 179 us
  Pallas kernels  117 us (65%)
  matrix products  55.1 us (31%)
  local copies, waits for them, and re-layouts  3.64 us (2%)
  other arithmetic  2.46 us (1%)
    pallas_call x1, Pallas kernels, dispatch(): pl.pallas_call(dispatch_kernel(senders, n_rows, capacity, col), out_shape...  70 us
    pallas_call x1, Pallas kernels, combine(): pl.pallas_call(combine_kernel(senders, n_rows, capacity, col), out_shape=...  37 us
    pallas_call x1, Pallas kernels, router_sum(): pl.pallas_call(body, out_shape=jax.ShapeDtypeStruct(terms.shape[1:], term...  9.63 us
    dot_general x1, matrix products, local(): lax.dot_general(output_rows, w_down, over_cols, preferred_element_type=jn...  8.16 us
    dot_general x1, matrix products, local(): lax.dot_general(hidden, out_scaled, over_rows, preferred_element_type=jnp...  7.82 us
    dot_general x1, matrix products, local(): lax.dot_general(up_back, w_up, over_cols, preferred_element_type=jnp.floa...  6.63 us
    dot_general x1, matrix products, local(): lax.dot_general(token_rows, gate_back, over_rows, preferred_element_type=...  6.02 us
    dot_general x1, matrix products, local(): up_pre = jnp.dot(token_rows, w_up, preferred_element_type=jnp.float32)  6.02 us

profile of v2, /device:TPU:0, one launch (start us, length us, event | category | flops | bytes accessed | tf_op | source)
XLA Modules:
  0.0 178.8 jit_solution(12291058014768783003)
XLA Ops:
  0.6 0.0 copy-start
  0.7 1.6 fusion.20
  2.3 0.7 select_reduce_fusion.3
  3.0 0.1 rev.6
  3.1 0.8 copy.42
  4.0 0.1 eq.44
  4.1 0.3 fusion.14
  4.4 0.1 convert_element_type.73
  4.5 0.1 copy.43
  4.6 0.7 add_bitcast_fusion
  5.3 0.3 select_reduce_fusion.1
  5.6 0.4 fusion.12
  6.0 1.5 copy.44
  7.6 0.0 copy-done
  7.6 0.0 copy-start.4
  7.6 0.4 convolution_convert_fusion.1
  8.0 0.7 convolution_convert_fusion
  8.8 70.0 %dispatch.1 = (bf16[1024,2048]{1,0:T(8,128)(2,1)S(1)}, bf16[1024,2048]{1,0:T(8,128)(2,1)S(1)}, f32[8,8,128]{2,1,0:T(8,128)S(1)}) custom-call(bf16[8,128,1024]{2,1,0:T(8,128)(2,1)S(1)} %bitcast.65, bf16[8,128,512]{2,1,0:T(8,128)(2,1)S(1)} %bitcast.66, f32[8,8,128]{2,1,0:T(8,128)S(1)} %pad.11.mix_ref), custom_call_target="tpu_custom_call" | custom-call | tf_op jit(solution)/shard_map/dispatch/pallas_call | solution.py:193
  78.8 0.0 copy-done.4
  78.8 0.0 copy-start.5
  78.8 4.2 %fusion.4 = f32[1024,896]{0,1:T(8,128)S(1)} fusion(bf16[1024,2048]{1,0:T(8,128)(2,1)S(1)} %get-tuple-element.13, bf16[1,2048,896]{2,1,0:T(8,128)(2,1)S(1)} %copy-done.4), kind=kOutput, calls=%fused_computation.6 | convolution fusion | flops 3758096384 | bytes 11534336 | tf_op jit(solution)/shard_map/dot_general | solution.py:457
  83.0 0.0 copy-done.5
  83.0 0.0 copy-start.3
  83.0 6.0 %fusion.7 = f32[1024,896]{0,1:T(8,128)} fusion(bf16[1024,2048]{1,0:T(8,128)(2,1)S(1)} %get-tuple-element.13, bf16[1,2048,896]{2,1,0:T(8,128)(2,1)S(1)} %copy-done.5), kind=kOutput, calls=%fused_computation.9 | convolution fusion | flops 3758096384 | bytes 11534336 | tf_op jit(solution)/shard_map/dot_general | solution.py:458
  89.0 0.0 copy-done.3
  89.0 8.2 %multiply_reduce_fusion = (f32[1024]{0:T(1024)S(1)}, bf16[1024,896]{0,1:T(8,128)(2,1)}, bf16[1024,896]{0,1:T(8,128)(2,1)S(1)}, bf16[1024,896]{0,1:T(8,128)(2,1)S(1)}) fusion(f32[1024,896]{0,1:T(8,128)} %fusion.7, f32[1024,896]{0,1:T(8,128)S(1)} %fusion.4, f32[1024]{0:T(1024)S(1)} %bitcast.81, bf16[1024,2048]{1,0:T(8,128)(2,1)S(1)} %get-tuple-element.12, ...), kind=kOutput, calls=%fused_computation.16 | convolution fusion | flops 3775527936 | bytes 20717568 | tf_op jit(solution)/shard_map/dot_general | solution.py:462
  97.2 0.0 copy-start.6
  97.2 7.8 %convert_bitcast_fusion = bf16[1,896,2048]{2,1,0:T(8,128)(2,1)} fusion(bf16[1024,896]{0,1:T(8,128)(2,1)} %get-tuple-element.17, bf16[1024,2048]{1,0:T(8,128)(2,1)S(1)} %get-tuple-element.12, f32[1024]{0:T(1024)S(1)} %bitcast.82), kind=kOutput, calls=%fused_computation.13 | convolution fusion | flops 3766222848 | bytes 9703424 | tf_op jit(solution)/shard_map/dot_general | solution.py:482
  105.0 6.0 %convert_bitcast_fusion.2 = bf16[1,2048,896]{2,1,0:T(8,128)(2,1)} fusion(bf16[1024,2048]{1,0:T(8,128)(2,1)S(1)} %get-tuple-element.13, bf16[1024,896]{0,1:T(8,128)(2,1)S(1)} %get-tuple-element.18), kind=kOutput, calls=%fused_computation.15 | convolution fusion | flops 3759931392 | bytes 9699328 | tf_op jit(solution)/shard_map/dot_general | solution.py:476
  111.1 0.0 copy-done.6
  111.1 6.0 %convert_bitcast_fusion.1 = bf16[1,2048,896]{2,1,0:T(8,128)(2,1)} fusion(bf16[1024,2048]{1,0:T(8,128)(2,1)S(1)} %get-tuple-element.13, bf16[1024,896]{0,1:T(8,128)(2,1)S(1)} %get-tuple-element.19), kind=kOutput, calls=%fused_computation.14 | convolution fusion | flops 3759931392 | bytes 9699328 | tf_op jit(solution)/shard_map/dot_general | solution.py:479
  117.1 4.6 %fusion.2 = f32[1024,2048]{1,0:T(8,128)S(1)} fusion(bf16[1024,896]{0,1:T(8,128)(2,1)S(1)} %get-tuple-element.18, bf16[1,2048,896]{2,1,0:T(8,128)(2,1)S(1)} %copy-done.4), kind=kOutput, calls=%fused_computation.4 | convolution fusion | flops 3758096384 | bytes 13893632 | tf_op jit(solution)/shard_map/dot_general | solution.py:472
  121.6 6.6 %add_convert_fusion = bf16[1024,2048]{1,0:T(8,128)(2,1)S(1)} fusion(f32[1024,2048]{1,0:T(8,128)S(1)} %fusion.2, bf16[1024,896]{0,1:T(8,128)(2,1)} %copy-done.6, bf16[1,2048,896]{2,1,0:T(8,128)(2,1)S(1)} %copy-done.5), kind=kOutput, calls=%fused_computation.1 | convolution fusion | flops 3762290688 | bytes 18087936 | tf_op jit(solution)/shard_map/dot_general | solution.py:473
  128.3 0.0 copy-start.1
  128.3 37.0 %combine.1 = (bf16[8,128,512]{2,1,0:T(8,128)(2,1)S(1)}, f32[8,8,128]{2,1,0:T(8,128)S(1)}) custom-call(bf16[8,128,2048]{2,1,0:T(8,128)(2,1)S(1)} %bitcast.67, f32[8,8,128]{2,1,0:T(8,128)S(1)} %pad.12.mix_ref), custom_call_target="tpu_custom_call" | custom-call | tf_op jit(solution)/shard_map/combine/pallas_call | solution.py:342
  165.3 0.3 select_reduce_fusion
  165.6 0.0 copy-start.2
  165.7 0.1 rev.7
  165.8 0.0 copy-done.1
  165.8 0.3 convolution_multiply_fusion
  166.1 0.1 reshape.67
  166.2 9.6 %router_sum.1 = f32[8,128]{1,0:T(8,128)S(1)} custom-call(f32[8,8,128]{2,1,0:T(8,128)S(1)} %pad.13.src), custom_call_target="tpu_custom_call" | custom-call | tf_op jit(solution)/shard_map/router_sum/pallas_call | solution.py:395
  175.8 0.6 slice_bitcast_fusion
  176.4 1.1 fusion.15
  177.6 1.2 fusion.13
  178.8 0.0 copy-done.2
  (13 shorter events, 0.1 us)
Async XLA Ops:
  0.6 6.9 %copy-start = (bf16[256,512]{1,0:T(8,128)(2,1)S(1)}, bf16[256,512]{1,0:T(8,128)(2,1)}, u32[]{:S(2)}) copy-start(bf16[256,512]{1,0:T(8,128)(2,1)} %param.10) | copy-start | bytes 786436
  7.6 71.2 %copy-start.4 = (bf16[1,2048,896]{2,1,0:T(8,128)(2,1)S(1)}, bf16[1,2048,896]{2,1,0:T(8,128)(2,1)}, u32[]{:S(2)}) copy-start(bf16[1,2048,896]{2,1,0:T(8,128)(2,1)} %param.11) | copy-start | bytes 11010052
  78.8 4.2 %copy-start.5 = (bf16[1,2048,896]{2,1,0:T(8,128)(2,1)S(1)}, bf16[1,2048,896]{2,1,0:T(8,128)(2,1)}, u32[]{:S(2)}) copy-start(bf16[1,2048,896]{2,1,0:T(8,128)(2,1)} %param.12) | copy-start | bytes 11010052
  83.0 6.0 %copy-start.3 = (bf16[1,896,2048]{2,1,0:T(8,128)(2,1)S(1)}, bf16[1,896,2048]{2,1,0:T(8,128)(2,1)}, u32[]{:S(2)}) copy-start(bf16[1,896,2048]{2,1,0:T(8,128)(2,1)} %param.13) | copy-start | bytes 11010052
  97.2 13.9 %copy-start.6 = (bf16[1024,896]{0,1:T(8,128)(2,1)}, bf16[1024,896]{0,1:T(8,128)(2,1)S(1)}, u32[]{:S(2)}) copy-start(bf16[1024,896]{0,1:T(8,128)(2,1)S(1)} %get-tuple-element.19) | copy-start | bytes 5505028
  128.3 37.5 %copy-start.1 = (s32[256,2]{0,1:T(2,128)S(1)}, s32[256,2]{0,1:T(2,128)}, u32[]{:S(2)}) copy-start(s32[256,2]{0,1:T(2,128)} %param.8) | copy-start | bytes 6148
  165.6 13.1 %copy-start.2 = (f32[2,256]{1,0:T(2,128)}, f32[2,256]{1,0:T(2,128)S(1)}, u32[]{:S(2)}) copy-start(f32[2,256]{1,0:T(2,128)S(1)} %select_reduce_fusion) | copy-start | bytes 6148

commit v3 on v2

--- a/solution.py
+++ b/solution.py
@@ -34,6 +34,19 @@
     return pair(me, k, size)
 
 
+def greet(me, tp, senders, peers):
+    barrier = pltpu.get_barrier_semaphore()
+
+    def hello(k, carry):
+        pl.semaphore_signal(barrier, inc=1, device_id=(pair(me, k, senders), tp), device_id_type=MESH)
+        return carry
+
+    lax.fori_loop(1, senders, hello, 0)
+    for peer in peers:
+        pl.semaphore_signal(barrier, inc=1, device_id=(me, peer), device_id_type=MESH)
+    pl.semaphore_wait(barrier, senders - 1 + len(peers))
+
+
 def span(start, size):
     return pl.ds(pl.multiple_of(start * size, size), size)
 
@@ -49,6 +62,8 @@
 
         def seat(step, side):
             return lax.rem(row + step + rows, rows) * 2 + side
+
+        greet(me, tp, senders, [partner] + [seat(j, core) for j in range(1, rows)])
 
         def piece(out, block, tp_col):
             return out.at[span(block, capacity), span(tp_col, col)]
@@ -202,7 +217,7 @@
             dma((senders,)), dma((senders,)),
             dma((3 + n_rows,)),
         ],
-        compiler_params=pltpu.CompilerParams(has_side_effects=True, vmem_limit_bytes=24 << 20),
+        compiler_params=pltpu.CompilerParams(has_side_effects=True, collective_id=0, vmem_limit_bytes=24 << 20),
         name="dispatch",
     )(tok_send, cot_send, mix_send)
 
@@ -218,6 +233,8 @@
 
         def seat(step, side):
             return lax.rem(row + step + rows, rows) * 2 + side
+
+        greet(me, tp, senders, [lax.rem(tp + k, 2 * rows) for k in range(1, 2 * rows)])
 
         def c_copy(step, block):
             return remote(terms.at[block, :, span(seat(step, 1 - core), col)], c_buf.at[step, block],
@@ -360,7 +377,7 @@
             dma((senders,)), dma((senders,)),
             dma((2 * n_rows,)), dma((2 * n_rows,)),
         ],
-        compiler_params=pltpu.CompilerParams(has_side_effects=True, vmem_limit_bytes=32 << 20),
+        compiler_params=pltpu.CompilerParams(has_side_effects=True, collective_id=1, vmem_limit_bytes=32 << 20),
         name="combine",
     )(terms, mix_part)
 
@@ -371,6 +388,8 @@
     def body(src, out, got, send, recv):
         me = lax.axis_index("ep")
         tp = lax.axis_index("tp")
+
+        greet(me, tp, senders, [])
 
         def copy(dest, slot):
             return remote(src.at[dest], got.at[slot], send.at[dest], recv.at[slot], dest, tp)
@@ -398,7 +417,7 @@
         in_specs=[vmem],
         out_specs=vmem,
         scratch_shapes=[pltpu.VMEM(terms.shape, terms.dtype), dma((senders,)), dma((senders,))],
-        compiler_params=pltpu.CompilerParams(has_side_effects=True, vmem_limit_bytes=8 << 20),
+        compiler_params=pltpu.CompilerParams(has_side_effects=True, collective_id=2, vmem_limit_bytes=8 << 20),
         name="router_sum",
     )(terms)
 

time: 179 us -> 170 us (0.950)
  Pallas kernels: 117 us -> 108 us
    pallas_call x1, Pallas kernels: 70 us -> 66.7 us  [dispatch(): pl.pallas_call(dispatch_kernel(senders, n_rows, capacity, col), out_shape...]
    pallas_call x1, Pallas kernels: 9.63 us -> 6.74 us  [router_sum(): pl.pallas_call(body, out_shape=jax.ShapeDtypeStruct(terms.shape[1:], term...]
    pallas_call x1, Pallas kernels: 37 us -> 34.4 us  [combine(): pl.pallas_call(combine_kernel(senders, n_rows, capacity, col), out_shape=...]
where the time goes in v3:
time: 170 us
  Pallas kernels  108 us (64%)
  matrix products  54.9 us (32%)
  local copies, waits for them, and re-layouts  3.64 us (2%)
  other arithmetic  2.46 us (1%)
    pallas_call x1, Pallas kernels, dispatch(): pl.pallas_call(dispatch_kernel(senders, n_rows, capacity, col), out_shape...  66.7 us
    pallas_call x1, Pallas kernels, combine(): pl.pallas_call(combine_kernel(senders, n_rows, capacity, col), out_shape=...  34.4 us
    dot_general x1, matrix products, local(): lax.dot_general(output_rows, w_down, over_cols, preferred_element_type=jn...  8.17 us
    dot_general x1, matrix products, local(): lax.dot_general(hidden, out_scaled, over_rows, preferred_element_type=jnp...  7.81 us
    pallas_call x1, Pallas kernels, router_sum(): pl.pallas_call(body, out_shape=jax.ShapeDtypeStruct(terms.shape[1:], term...  6.74 us
    dot_general x1, matrix products, local(): lax.dot_general(up_back, w_up, over_cols, preferred_element_type=jnp.floa...  6.37 us
    dot_general x1, matrix products, local(): lax.dot_general(token_rows, gate_back, over_rows, preferred_element_type=...  6.02 us
    dot_general x1, matrix products, local(): up_pre = jnp.dot(token_rows, w_up, preferred_element_type=jnp.float32)  6.02 us

profile of v3, /device:TPU:0, one launch (start us, length us, event | category | flops | bytes accessed | tf_op | source)
XLA Modules:
  0.0 169.8 jit_solution(4546116727913991309)
XLA Ops:
  0.6 0.0 copy-start
  0.7 1.6 fusion.20
  2.3 0.7 select_reduce_fusion.3
  3.0 0.1 rev.6
  3.1 0.8 copy.42
  4.0 0.1 eq.44
  4.1 0.3 fusion.14
  4.4 0.1 convert_element_type.73
  4.5 0.1 copy.43
  4.6 0.7 add_bitcast_fusion
  5.3 0.3 select_reduce_fusion.1
  5.6 0.4 fusion.12
  6.0 1.5 copy.44
  7.6 0.0 copy-done
  7.6 0.0 copy-start.4
  7.6 0.4 convolution_convert_fusion.1
  8.0 0.7 convolution_convert_fusion
  8.8 66.7 %dispatch.1 = (bf16[1024,2048]{1,0:T(8,128)(2,1)S(1)}, bf16[1024,2048]{1,0:T(8,128)(2,1)S(1)}, f32[8,8,128]{2,1,0:T(8,128)S(1)}) custom-call(bf16[8,128,1024]{2,1,0:T(8,128)(2,1)S(1)} %bitcast.65, bf16[8,128,512]{2,1,0:T(8,128)(2,1)S(1)} %bitcast.66, f32[8,8,128]{2,1,0:T(8,128)S(1)} %pad.11.mix_ref), custom_call_target="tpu_custom_call" | custom-call | tf_op jit(solution)/shard_map/dispatch/pallas_call | solution.py:208
  75.5 0.0 copy-done.4
  75.6 0.0 copy-start.5
  75.6 4.2 %fusion.4 = f32[1024,896]{0,1:T(8,128)S(1)} fusion(bf16[1024,2048]{1,0:T(8,128)(2,1)S(1)} %get-tuple-element.13, bf16[1,2048,896]{2,1,0:T(8,128)(2,1)S(1)} %copy-done.4), kind=kOutput, calls=%fused_computation.6 | convolution fusion | flops 3758096384 | bytes 11534336 | tf_op jit(solution)/shard_map/dot_general | solution.py:476
  79.8 0.0 copy-done.5
  79.8 0.0 copy-start.3
  79.8 6.0 %fusion.7 = f32[1024,896]{0,1:T(8,128)} fusion(bf16[1024,2048]{1,0:T(8,128)(2,1)S(1)} %get-tuple-element.13, bf16[1,2048,896]{2,1,0:T(8,128)(2,1)S(1)} %copy-done.5), kind=kOutput, calls=%fused_computation.9 | convolution fusion | flops 3758096384 | bytes 11534336 | tf_op jit(solution)/shard_map/dot_general | solution.py:477
  85.8 0.0 copy-done.3
  85.8 8.2 %multiply_reduce_fusion = (f32[1024]{0:T(1024)S(1)}, bf16[1024,896]{0,1:T(8,128)(2,1)}, bf16[1024,896]{0,1:T(8,128)(2,1)S(1)}, bf16[1024,896]{0,1:T(8,128)(2,1)S(1)}) fusion(f32[1024,896]{0,1:T(8,128)} %fusion.7, f32[1024,896]{0,1:T(8,128)S(1)} %fusion.4, f32[1024]{0:T(1024)S(1)} %bitcast.81, bf16[1024,2048]{1,0:T(8,128)(2,1)S(1)} %get-tuple-element.12, ...), kind=kOutput, calls=%fused_computation.16 | convolution fusion | flops 3775527936 | bytes 20717568 | tf_op jit(solution)/shard_map/dot_general | solution.py:481
  94.0 0.0 copy-start.6
  94.0 7.8 %convert_bitcast_fusion = bf16[1,896,2048]{2,1,0:T(8,128)(2,1)} fusion(bf16[1024,896]{0,1:T(8,128)(2,1)} %get-tuple-element.17, bf16[1024,2048]{1,0:T(8,128)(2,1)S(1)} %get-tuple-element.12, f32[1024]{0:T(1024)S(1)} %bitcast.82), kind=kOutput, calls=%fused_computation.13 | convolution fusion | flops 3766222848 | bytes 9703424 | tf_op jit(solution)/shard_map/dot_general | solution.py:501
  101.8 6.0 %convert_bitcast_fusion.2 = bf16[1,2048,896]{2,1,0:T(8,128)(2,1)} fusion(bf16[1024,2048]{1,0:T(8,128)(2,1)S(1)} %get-tuple-element.13, bf16[1024,896]{0,1:T(8,128)(2,1)S(1)} %get-tuple-element.18), kind=kOutput, calls=%fused_computation.15 | convolution fusion | flops 3759931392 | bytes 9699328 | tf_op jit(solution)/shard_map/dot_general | solution.py:495
  107.8 0.0 copy-done.6
  107.8 6.0 %convert_bitcast_fusion.1 = bf16[1,2048,896]{2,1,0:T(8,128)(2,1)} fusion(bf16[1024,2048]{1,0:T(8,128)(2,1)S(1)} %get-tuple-element.13, bf16[1024,896]{0,1:T(8,128)(2,1)S(1)} %get-tuple-element.19), kind=kOutput, calls=%fused_computation.14 | convolution fusion | flops 3759931392 | bytes 9699328 | tf_op jit(solution)/shard_map/dot_general | solution.py:498
  113.8 4.6 %fusion.2 = f32[1024,2048]{1,0:T(8,128)S(1)} fusion(bf16[1024,896]{0,1:T(8,128)(2,1)S(1)} %get-tuple-element.18, bf16[1,2048,896]{2,1,0:T(8,128)(2,1)S(1)} %copy-done.4), kind=kOutput, calls=%fused_computation.4 | convolution fusion | flops 3758096384 | bytes 13893632 | tf_op jit(solution)/shard_map/dot_general | solution.py:491
  118.4 6.4 %add_convert_fusion = bf16[1024,2048]{1,0:T(8,128)(2,1)S(1)} fusion(f32[1024,2048]{1,0:T(8,128)S(1)} %fusion.2, bf16[1024,896]{0,1:T(8,128)(2,1)} %copy-done.6, bf16[1,2048,896]{2,1,0:T(8,128)(2,1)S(1)} %copy-done.5), kind=kOutput, calls=%fused_computation.1 | convolution fusion | flops 3762290688 | bytes 18087936 | tf_op jit(solution)/shard_map/dot_general | solution.py:492
  124.8 0.0 copy-start.1
  124.8 34.4 %combine.1 = (bf16[8,128,512]{2,1,0:T(8,128)(2,1)S(1)}, f32[8,8,128]{2,1,0:T(8,128)S(1)}) custom-call(bf16[8,128,2048]{2,1,0:T(8,128)(2,1)S(1)} %bitcast.67, f32[8,8,128]{2,1,0:T(8,128)S(1)} %pad.12.mix_ref), custom_call_target="tpu_custom_call" | custom-call | tf_op jit(solution)/shard_map/combine/pallas_call | solution.py:359
  159.3 0.3 select_reduce_fusion
  159.6 0.0 copy-start.2
  159.6 0.1 rev.7
  159.7 0.0 copy-done.1
  159.7 0.3 convolution_multiply_fusion
  160.0 0.1 reshape.67
  160.2 6.7 %router_sum.1 = f32[8,128]{1,0:T(8,128)S(1)} custom-call(f32[8,8,128]{2,1,0:T(8,128)S(1)} %pad.13.src), custom_call_target="tpu_custom_call" | custom-call | tf_op jit(solution)/shard_map/router_sum/pallas_call | solution.py:414
  166.9 0.6 slice_bitcast_fusion
  167.5 1.1 fusion.15
  168.6 1.2 fusion.13
  169.8 0.0 copy-done.2
  (13 shorter events, 0.1 us)
Async XLA Ops:
  0.6 6.9 %copy-start = (bf16[256,512]{1,0:T(8,128)(2,1)S(1)}, bf16[256,512]{1,0:T(8,128)(2,1)}, u32[]{:S(2)}) copy-start(bf16[256,512]{1,0:T(8,128)(2,1)} %param.10) | copy-start | bytes 786436
  7.6 68.0 %copy-start.4 = (bf16[1,2048,896]{2,1,0:T(8,128)(2,1)S(1)}, bf16[1,2048,896]{2,1,0:T(8,128)(2,1)}, u32[]{:S(2)}) copy-start(bf16[1,2048,896]{2,1,0:T(8,128)(2,1)} %param.11) | copy-start | bytes 11010052
  75.6 4.2 %copy-start.5 = (bf16[1,2048,896]{2,1,0:T(8,128)(2,1)S(1)}, bf16[1,2048,896]{2,1,0:T(8,128)(2,1)}, u32[]{:S(2)}) copy-start(bf16[1,2048,896]{2,1,0:T(8,128)(2,1)} %param.12) | copy-start | bytes 11010052
  79.8 6.0 %copy-start.3 = (bf16[1,896,2048]{2,1,0:T(8,128)(2,1)S(1)}, bf16[1,896,2048]{2,1,0:T(8,128)(2,1)}, u32[]{:S(2)}) copy-start(bf16[1,896,2048]{2,1,0:T(8,128)(2,1)} %param.13) | copy-start | bytes 11010052
  94.0 13.8 %copy-start.6 = (bf16[1024,896]{0,1:T(8,128)(2,1)}, bf16[1024,896]{0,1:T(8,128)(2,1)S(1)}, u32[]{:S(2)}) copy-start(bf16[1024,896]{0,1:T(8,128)(2,1)S(1)} %get-tuple-element.19) | copy-start | bytes 5505028
  124.8 34.9 %copy-start.1 = (s32[256,2]{0,1:T(2,128)S(1)}, s32[256,2]{0,1:T(2,128)}, u32[]{:S(2)}) copy-start(s32[256,2]{0,1:T(2,128)} %param.8) | copy-start | bytes 6148
  159.6 10.2 %copy-start.2 = (f32[2,256]{1,0:T(2,128)}, f32[2,256]{1,0:T(2,128)S(1)}, u32[]{:S(2)}) copy-start(f32[2,256]{1,0:T(2,128)S(1)} %select_reduce_fusion) | copy-start | bytes 6148
